TPU v7x, 128 devices: a whole 4x4x4 slice. The times are simulated.
128 devices in a mesh: sp: 32 (over z, y, core), tp: 4 (over x).
Axes of the slice: x: 4, y: 4, z: 4, core: 2. Of those that a mesh axis runs over, the one named last changes fastest.
Arguments:
- tokens: bfloat16 [16384, 2048], P(('sp', 'tp')), may hold values from -6 to 6
- queries: bfloat16 [16384, 1024], P('sp', 'tp'), may hold values from -160 to 160
- keys: bfloat16 [16384, 1024], P('sp', 'tp'), may hold values from -8 to 8
- values: bfloat16 [16384, 1024], P('sp', 'tp'), may hold values from -6 to 6
- lambdas: float32 [8], P('tp'), may hold values from 0.3 to 0.8
- head_gain: float32 [128], replicated, may hold values from 0.1 to 1.9
- out_weight: bfloat16 [1024, 2048], replicated, may hold values from -0.1875 to 0.1875
- mixer_gain: float32 [2048], replicated, may hold values from 0.1 to 1.9
- up_weight: bfloat16 [2048, 4096], P('sp', 'tp'), may hold values from -0.125 to 0.125
- down_weight: bfloat16 [4096, 2048], P('tp', 'sp'), may hold values from -0.09375 to 0.09375
Outputs:
- result: bfloat16 [16384, 2048], P(('sp', 'tp'))
All inputs are finite; a program needn't handle non-finite values.
Results may differ from a plain program's by a relative error of at most 0.02.
Values may be sent and summed in bfloat16 or wider, within the bound.
A program may use at most 128 MiB of HBM per device.

v0:
```python
import math

import jax
import jax.numpy as jnp
from jax import lax
from jax.sharding import PartitionSpec as P

DQK = 64
DV = 128


def sent_together(arrays, axis, dim, along):
    both = jnp.concatenate(arrays, axis=along)
    whole, at, done = (lax.all_gather(both, axis, axis=dim, tiled=True), 0, [])
    for a in arrays:
        done.append(lax.slice_in_dim(whole, at, at + a.shape[along], axis=along))
        at += a.shape[along]
    return tuple(done)


def laid_out(pieces, dim):
    pieces = jnp.moveaxis(pieces, 0, dim)
    dims = pieces.shape
    return pieces.reshape(*dims[:dim], dims[dim] * dims[dim + 1], *dims[dim + 2 :])


def from_everyone(array, axis):
    count = lax.axis_size(axis)
    return lax.all_to_all(
        jnp.broadcast_to(array[None], (count, *array.shape)), axis, 0, 0, tiled=True
    )


def gathered_copies(array, axis, dim):
    return laid_out(from_everyone(array, axis), dim)


def cut_along(array, dim, count):
    dims = array.shape
    pieces = array.reshape(*dims[:dim], count, dims[dim] // count, *dims[dim + 1 :])
    return jnp.moveaxis(pieces, dim, 0)


def sum_at_owner(array, axis, dim):
    count = lax.axis_size(axis)
    pieces = lax.all_to_all(cut_along(array, dim, count), axis, 0, 0, tiled=True)
    return jnp.sum(pieces.astype(jnp.float32), axis=0)


def per_device(
    tokens,
    queries,
    keys,
    values,
    lambdas,
    head_gain,
    out_weight,
    mixer_gain,
    up_weight,
    down_weight,
):
    tok_rows = queries.shape[0]
    head_count = lambdas.shape[0]
    scaling = DQK ** (-0.5)
    sp_index = lax.axis_index("sp")
    first_row = sp_index * tok_rows
    last_row = first_row + tok_rows - 1
    query_split = queries.reshape(tok_rows, head_count, 2, DQK)
    query_pos = first_row + lax.broadcasted_iota(jnp.int32, (tok_rows, 1), 0)
    floor_max = jnp.full((head_count, tok_rows), -1e30, jnp.float32)
    zero_total = jnp.zeros((head_count, tok_rows), jnp.float32)
    zero_acc = jnp.zeros((head_count, tok_rows, DV), jnp.float32)
    start_state = (floor_max, zero_total, zero_acc, floor_max, zero_total, zero_acc)
    pieces = sent_together((keys, values), "sp", 0, 1)
    key_piece = pieces[0]
    value_piece = pieces[1]
    piece_rows = key_piece.shape[0]
    block_width = math.gcd(piece_rows, 512)

    def one_block(block_index, running):
        offset = block_index * block_width

        def update(inner):
            key_block = lax.dynamic_slice_in_dim(key_piece, offset, block_width, 0).reshape(
                block_width, head_count, 2, DQK
            )
            value_block = lax.dynamic_slice_in_dim(value_piece, offset, block_width, 0).reshape(
                block_width, head_count, DV
            )
            key_pos = offset + lax.broadcasted_iota(jnp.int32, (1, block_width), 1)
            allowed = key_pos <= query_pos
            updated = []
            for map_index in range(2):
                run_max = inner[3 * map_index]
                run_total = inner[3 * map_index + 1]
                run_acc = inner[3 * map_index + 2]
                scores = (
                    jnp.einsum(
                        "qhd,khd->hqk",
                        query_split[:, :, map_index],
                        key_block[:, :, map_index],
                        preferred_element_type=jnp.float32,
                    )
                    * scaling
                )
                scores = jnp.where(allowed[None], scores, -jnp.inf)
                new_max = jnp.maximum(run_max, jnp.max(scores, axis=2))
                shrink = jnp.exp(run_max - new_max)
                exponent = jnp.exp(scores - new_max[:, :, None])
                new_total = run_total * shrink + jnp.sum(exponent, axis=2)
                new_acc = run_acc * shrink[:, :, None] + jnp.einsum(
                    "hqk,khd->hqd",
                    exponent.astype(jnp.bfloat16),
                    value_block,
                    preferred_element_type=jnp.float32,
                )
                updated += [new_max, new_total, new_acc]
            return tuple(updated)

        return lax.cond(offset <= last_row, update, lambda inner: inner, running)

    final = lax.fori_loop(0, piece_rows // block_width, one_block, start_state)
    first_map = final[2] / final[1][:, :, None]
    second_map = final[5] / final[4][:, :, None]
    differ = first_map - lambdas[:, None, None] * second_map
    spread = lax.rsqrt(jnp.mean(differ * differ, axis=2, keepdims=True) + 1e-06)
    attended = (differ * spread * head_gain).astype(jnp.bfloat16)
    attended = jnp.transpose(attended, (1, 0, 2)).reshape(tok_rows, head_count * DV)
    all_heads = lax.all_to_all(attended, "tp", split_axis=0, concat_axis=1, tiled=True)
    projected = jnp.dot(all_heads, out_weight, preferred_element_type=jnp.float32).astype(
        jnp.bfloat16
    )
    resid = (tokens.astype(jnp.float32) + projected.astype(jnp.float32)).astype(jnp.bfloat16)
    resid_full = resid.astype(jnp.float32)
    normed = (
        resid_full
        * lax.rsqrt(jnp.mean(resid_full * resid_full, axis=1, keepdims=True) + 1e-06)
        * mixer_gain
    ).astype(jnp.bfloat16)
    up_full, down_full = (
        lax.all_gather(up_weight, "sp", axis=0, tiled=True),
        lax.all_gather(down_weight, "sp", axis=1, tiled=True),
    )
    hidden = jnp.square(
        jax.nn.relu(
            jnp.dot(gathered_copies(normed, "tp", 0), up_full, preferred_element_type=jnp.float32)
        )
    ).astype(jnp.bfloat16)
    mixed = sum_at_owner(
        jnp.dot(hidden, down_full, preferred_element_type=jnp.float32).astype(jnp.bfloat16), "tp", 0
    )
    return (resid_full + mixed).astype(jnp.bfloat16)


def solution(mesh):
    placed = (
        P(("sp", "tp"), None),
        P("sp", "tp"),
        P("sp", "tp"),
        P("sp", "tp"),
        P("tp"),
        P(),
        P(),
        P(),
        P("sp", "tp"),
        P("tp", "sp"),
    )
    return jax.shard_map(
        per_device, mesh=mesh, in_specs=placed, out_specs=P(("sp", "tp"), None), check_vma=False
    )
```

profile of v0, /device:TPU:121, one launch (start us, length us, event | category | flops | bytes accessed | tf_op | source)
XLA Modules:
  0.0 368.8 jit_solution(13263718865598575634)
XLA Ops:
  11.3 78.2 %all-gather.4.cloned.1.call-done = bf16[16384,512]{0,1:T(8,128)(2,1)} async-done(((bf16[512,512]{0,1:T(8,128)(2,1)}), bf16[16384,512]{0,1:T(8,128)(2,1)}) %all-gather.4.cloned.1.call-update) | async-done | bytes 16777232 | tf_op jit(solution)/shard_map/all_gather | solution.py:14
  89.5 11.4 %fusion.22 = (bf16[16384,256]{0,1:T(8,128)(2,1)}, bf16[16384,256]{0,1:T(8,128)(2,1)}) fusion(bf16[16384,512]{0,1:T(8,128)(2,1)} %all-gather.4.cloned.1.call-done), kind=kLoop, calls=%fused_computation.49 | loop fusion | bytes 33554432 | tf_op jit(solution)/shard_map/slice | solution.py:16
  101.1 180.4 %while.24 = (s32[]{:T(128)}, f32[2,512]{1,0:T(2,128)S(1)}, f32[2,512]{1,0:T(2,128)S(1)}, f32[2,512,128]{2,1,0:T(8,128)S(1)}, f32[2,512]{1,0:T(2,128)S(1)}, /*ind...) while((s32[]{:T(128)}, f32[2,512]{1,0:T(2,128)S(1)}, ...), condition=%wide.region_7.8_spmd.clone, body=%wide.region_0.7_spmd.clone.sunk | while | flops 410784768 | bytes 17707416 | solution.py:122
  112.4 5.6 %conditional.3 = ((f32[2,512]{1,0:T(2,128)S(1)}, f32[2,512]{1,0:T(2,128)S(1)}, f32[2,512,128]{2,1,0:T(8,128)S(1)}, f32[2,512]{1,0:T(2,128)S(1)}, f32[2,512]{1,0:T(2,128)S(1)}, /*index=5*/f32[2,512,128]{2,1,0:T(8,128)S(1)})) conditional(s32[]{:T(128)} %convert_element_type.94, (f32[2,512]{1,0:T(2,128)S(1)}, f32[2,512]{1,0:T(2,128)S(1)}, ...), branch_computations={%region_1.0_spmd, %region_2.6_spmd} | conditional | flops 410784768 | bytes 17705066 | solution.py:120
  118.0 5.6 %conditional.3 = ((f32[2,512]{1,0:T(2,128)S(1)}, f32[2,512]{1,0:T(2,128)S(1)}, f32[2,512,128]{2,1,0:T(8,128)S(1)}, f32[2,512]{1,0:T(2,128)S(1)}, f32[2,512]{1,0:T(2,128)S(1)}, /*index=5*/f32[2,512,128]{2,1,0:T(8,128)S(1)})) conditional(s32[]{:T(128)} %convert_element_type.94, (f32[2,512]{1,0:T(2,128)S(1)}, f32[2,512]{1,0:T(2,128)S(1)}, ...), branch_computations={%region_1.0_spmd, %region_2.6_spmd} | conditional | flops 410784768 | bytes 17705066 | solution.py:120
  123.7 5.6 %conditional.3 = ((f32[2,512]{1,0:T(2,128)S(1)}, f32[2,512]{1,0:T(2,128)S(1)}, f32[2,512,128]{2,1,0:T(8,128)S(1)}, f32[2,512]{1,0:T(2,128)S(1)}, f32[2,512]{1,0:T(2,128)S(1)}, /*index=5*/f32[2,512,128]{2,1,0:T(8,128)S(1)})) conditional(s32[]{:T(128)} %convert_element_type.94, (f32[2,512]{1,0:T(2,128)S(1)}, f32[2,512]{1,0:T(2,128)S(1)}, ...), branch_computations={%region_1.0_spmd, %region_2.6_spmd} | conditional | flops 410784768 | bytes 17705066 | solution.py:120
  140.6 5.6 %conditional.3 = ((f32[2,512]{1,0:T(2,128)S(1)}, f32[2,512]{1,0:T(2,128)S(1)}, f32[2,512,128]{2,1,0:T(8,128)S(1)}, f32[2,512]{1,0:T(2,128)S(1)}, f32[2,512]{1,0:T(2,128)S(1)}, /*index=5*/f32[2,512,128]{2,1,0:T(8,128)S(1)})) conditional(s32[]{:T(128)} %convert_element_type.94, (f32[2,512]{1,0:T(2,128)S(1)}, f32[2,512]{1,0:T(2,128)S(1)}, ...), branch_computations={%region_1.0_spmd, %region_2.6_spmd} | conditional | flops 410784768 | bytes 17705066 | solution.py:120
  146.2 5.6 %conditional.3 = ((f32[2,512]{1,0:T(2,128)S(1)}, f32[2,512]{1,0:T(2,128)S(1)}, f32[2,512,128]{2,1,0:T(8,128)S(1)}, f32[2,512]{1,0:T(2,128)S(1)}, f32[2,512]{1,0:T(2,128)S(1)}, /*index=5*/f32[2,512,128]{2,1,0:T(8,128)S(1)})) conditional(s32[]{:T(128)} %convert_element_type.94, (f32[2,512]{1,0:T(2,128)S(1)}, f32[2,512]{1,0:T(2,128)S(1)}, ...), branch_computations={%region_1.0_spmd, %region_2.6_spmd} | conditional | flops 410784768 | bytes 17705066 | solution.py:120
  151.9 5.6 %conditional.3 = ((f32[2,512]{1,0:T(2,128)S(1)}, f32[2,512]{1,0:T(2,128)S(1)}, f32[2,512,128]{2,1,0:T(8,128)S(1)}, f32[2,512]{1,0:T(2,128)S(1)}, f32[2,512]{1,0:T(2,128)S(1)}, /*index=5*/f32[2,512,128]{2,1,0:T(8,128)S(1)})) conditional(s32[]{:T(128)} %convert_element_type.94, (f32[2,512]{1,0:T(2,128)S(1)}, f32[2,512]{1,0:T(2,128)S(1)}, ...), branch_computations={%region_1.0_spmd, %region_2.6_spmd} | conditional | flops 410784768 | bytes 17705066 | solution.py:120
  157.5 5.6 %conditional.3 = ((f32[2,512]{1,0:T(2,128)S(1)}, f32[2,512]{1,0:T(2,128)S(1)}, f32[2,512,128]{2,1,0:T(8,128)S(1)}, f32[2,512]{1,0:T(2,128)S(1)}, f32[2,512]{1,0:T(2,128)S(1)}, /*index=5*/f32[2,512,128]{2,1,0:T(8,128)S(1)})) conditional(s32[]{:T(128)} %convert_element_type.94, (f32[2,512]{1,0:T(2,128)S(1)}, f32[2,512]{1,0:T(2,128)S(1)}, ...), branch_computations={%region_1.0_spmd, %region_2.6_spmd} | conditional | flops 410784768 | bytes 17705066 | solution.py:120
  163.1 5.6 %conditional.3 = ((f32[2,512]{1,0:T(2,128)S(1)}, f32[2,512]{1,0:T(2,128)S(1)}, f32[2,512,128]{2,1,0:T(8,128)S(1)}, f32[2,512]{1,0:T(2,128)S(1)}, f32[2,512]{1,0:T(2,128)S(1)}, /*index=5*/f32[2,512,128]{2,1,0:T(8,128)S(1)})) conditional(s32[]{:T(128)} %convert_element_type.94, (f32[2,512]{1,0:T(2,128)S(1)}, f32[2,512]{1,0:T(2,128)S(1)}, ...), branch_computations={%region_1.0_spmd, %region_2.6_spmd} | conditional | flops 410784768 | bytes 17705066 | solution.py:120
  168.8 5.6 %conditional.3 = ((f32[2,512]{1,0:T(2,128)S(1)}, f32[2,512]{1,0:T(2,128)S(1)}, f32[2,512,128]{2,1,0:T(8,128)S(1)}, f32[2,512]{1,0:T(2,128)S(1)}, f32[2,512]{1,0:T(2,128)S(1)}, /*index=5*/f32[2,512,128]{2,1,0:T(8,128)S(1)})) conditional(s32[]{:T(128)} %convert_element_type.94, (f32[2,512]{1,0:T(2,128)S(1)}, f32[2,512]{1,0:T(2,128)S(1)}, ...), branch_computations={%region_1.0_spmd, %region_2.6_spmd} | conditional | flops 410784768 | bytes 17705066 | solution.py:120
  174.4 5.7 %conditional.3 = ((f32[2,512]{1,0:T(2,128)S(1)}, f32[2,512]{1,0:T(2,128)S(1)}, f32[2,512,128]{2,1,0:T(8,128)S(1)}, f32[2,512]{1,0:T(2,128)S(1)}, f32[2,512]{1,0:T(2,128)S(1)}, /*index=5*/f32[2,512,128]{2,1,0:T(8,128)S(1)})) conditional(s32[]{:T(128)} %convert_element_type.94, (f32[2,512]{1,0:T(2,128)S(1)}, f32[2,512]{1,0:T(2,128)S(1)}, ...), branch_computations={%region_1.0_spmd, %region_2.6_spmd} | conditional | flops 410784768 | bytes 17705066 | solution.py:120
  180.1 5.6 %conditional.3 = ((f32[2,512]{1,0:T(2,128)S(1)}, f32[2,512]{1,0:T(2,128)S(1)}, f32[2,512,128]{2,1,0:T(8,128)S(1)}, f32[2,512]{1,0:T(2,128)S(1)}, f32[2,512]{1,0:T(2,128)S(1)}, /*index=5*/f32[2,512,128]{2,1,0:T(8,128)S(1)})) conditional(s32[]{:T(128)} %convert_element_type.94, (f32[2,512]{1,0:T(2,128)S(1)}, f32[2,512]{1,0:T(2,128)S(1)}, ...), branch_computations={%region_1.0_spmd, %region_2.6_spmd} | conditional | flops 410784768 | bytes 17705066 | solution.py:120
  191.4 5.6 %conditional.3 = ((f32[2,512]{1,0:T(2,128)S(1)}, f32[2,512]{1,0:T(2,128)S(1)}, f32[2,512,128]{2,1,0:T(8,128)S(1)}, f32[2,512]{1,0:T(2,128)S(1)}, f32[2,512]{1,0:T(2,128)S(1)}, /*index=5*/f32[2,512,128]{2,1,0:T(8,128)S(1)})) conditional(s32[]{:T(128)} %convert_element_type.94, (f32[2,512]{1,0:T(2,128)S(1)}, f32[2,512]{1,0:T(2,128)S(1)}, ...), branch_computations={%region_1.0_spmd, %region_2.6_spmd} | conditional | flops 410784768 | bytes 17705066 | solution.py:120
  197.0 5.6 %conditional.3 = ((f32[2,512]{1,0:T(2,128)S(1)}, f32[2,512]{1,0:T(2,128)S(1)}, f32[2,512,128]{2,1,0:T(8,128)S(1)}, f32[2,512]{1,0:T(2,128)S(1)}, f32[2,512]{1,0:T(2,128)S(1)}, /*index=5*/f32[2,512,128]{2,1,0:T(8,128)S(1)})) conditional(s32[]{:T(128)} %convert_element_type.94, (f32[2,512]{1,0:T(2,128)S(1)}, f32[2,512]{1,0:T(2,128)S(1)}, ...), branch_computations={%region_1.0_spmd, %region_2.6_spmd} | conditional | flops 410784768 | bytes 17705066 | solution.py:120
  202.7 5.6 %conditional.3 = ((f32[2,512]{1,0:T(2,128)S(1)}, f32[2,512]{1,0:T(2,128)S(1)}, f32[2,512,128]{2,1,0:T(8,128)S(1)}, f32[2,512]{1,0:T(2,128)S(1)}, f32[2,512]{1,0:T(2,128)S(1)}, /*index=5*/f32[2,512,128]{2,1,0:T(8,128)S(1)})) conditional(s32[]{:T(128)} %convert_element_type.94, (f32[2,512]{1,0:T(2,128)S(1)}, f32[2,512]{1,0:T(2,128)S(1)}, ...), branch_computations={%region_1.0_spmd, %region_2.6_spmd} | conditional | flops 410784768 | bytes 17705066 | solution.py:120
  208.3 5.6 %conditional.3 = ((f32[2,512]{1,0:T(2,128)S(1)}, f32[2,512]{1,0:T(2,128)S(1)}, f32[2,512,128]{2,1,0:T(8,128)S(1)}, f32[2,512]{1,0:T(2,128)S(1)}, f32[2,512]{1,0:T(2,128)S(1)}, /*index=5*/f32[2,512,128]{2,1,0:T(8,128)S(1)})) conditional(s32[]{:T(128)} %convert_element_type.94, (f32[2,512]{1,0:T(2,128)S(1)}, f32[2,512]{1,0:T(2,128)S(1)}, ...), branch_computations={%region_1.0_spmd, %region_2.6_spmd} | conditional | flops 410784768 | bytes 17705066 | solution.py:120
  213.9 5.6 %conditional.3 = ((f32[2,512]{1,0:T(2,128)S(1)}, f32[2,512]{1,0:T(2,128)S(1)}, f32[2,512,128]{2,1,0:T(8,128)S(1)}, f32[2,512]{1,0:T(2,128)S(1)}, f32[2,512]{1,0:T(2,128)S(1)}, /*index=5*/f32[2,512,128]{2,1,0:T(8,128)S(1)})) conditional(s32[]{:T(128)} %convert_element_type.94, (f32[2,512]{1,0:T(2,128)S(1)}, f32[2,512]{1,0:T(2,128)S(1)}, ...), branch_computations={%region_1.0_spmd, %region_2.6_spmd} | conditional | flops 410784768 | bytes 17705066 | solution.py:120
  219.6 5.6 %conditional.3 = ((f32[2,512]{1,0:T(2,128)S(1)}, f32[2,512]{1,0:T(2,128)S(1)}, f32[2,512,128]{2,1,0:T(8,128)S(1)}, f32[2,512]{1,0:T(2,128)S(1)}, f32[2,512]{1,0:T(2,128)S(1)}, /*index=5*/f32[2,512,128]{2,1,0:T(8,128)S(1)})) conditional(s32[]{:T(128)} %convert_element_type.94, (f32[2,512]{1,0:T(2,128)S(1)}, f32[2,512]{1,0:T(2,128)S(1)}, ...), branch_computations={%region_1.0_spmd, %region_2.6_spmd} | conditional | flops 410784768 | bytes 17705066 | solution.py:120
  225.2 5.6 %conditional.3 = ((f32[2,512]{1,0:T(2,128)S(1)}, f32[2,512]{1,0:T(2,128)S(1)}, f32[2,512,128]{2,1,0:T(8,128)S(1)}, f32[2,512]{1,0:T(2,128)S(1)}, f32[2,512]{1,0:T(2,128)S(1)}, /*index=5*/f32[2,512,128]{2,1,0:T(8,128)S(1)})) conditional(s32[]{:T(128)} %convert_element_type.94, (f32[2,512]{1,0:T(2,128)S(1)}, f32[2,512]{1,0:T(2,128)S(1)}, ...), branch_computations={%region_1.0_spmd, %region_2.6_spmd} | conditional | flops 410784768 | bytes 17705066 | solution.py:120
  230.8 5.6 %conditional.3 = ((f32[2,512]{1,0:T(2,128)S(1)}, f32[2,512]{1,0:T(2,128)S(1)}, f32[2,512,128]{2,1,0:T(8,128)S(1)}, f32[2,512]{1,0:T(2,128)S(1)}, f32[2,512]{1,0:T(2,128)S(1)}, /*index=5*/f32[2,512,128]{2,1,0:T(8,128)S(1)})) conditional(s32[]{:T(128)} %convert_element_type.94, (f32[2,512]{1,0:T(2,128)S(1)}, f32[2,512]{1,0:T(2,128)S(1)}, ...), branch_computations={%region_1.0_spmd, %region_2.6_spmd} | conditional | flops 410784768 | bytes 17705066 | solution.py:120
  236.5 5.6 %conditional.3 = ((f32[2,512]{1,0:T(2,128)S(1)}, f32[2,512]{1,0:T(2,128)S(1)}, f32[2,512,128]{2,1,0:T(8,128)S(1)}, f32[2,512]{1,0:T(2,128)S(1)}, f32[2,512]{1,0:T(2,128)S(1)}, /*index=5*/f32[2,512,128]{2,1,0:T(8,128)S(1)})) conditional(s32[]{:T(128)} %convert_element_type.94, (f32[2,512]{1,0:T(2,128)S(1)}, f32[2,512]{1,0:T(2,128)S(1)}, ...), branch_computations={%region_1.0_spmd, %region_2.6_spmd} | conditional | flops 410784768 | bytes 17705066 | solution.py:120
  242.1 5.6 %conditional.3 = ((f32[2,512]{1,0:T(2,128)S(1)}, f32[2,512]{1,0:T(2,128)S(1)}, f32[2,512,128]{2,1,0:T(8,128)S(1)}, f32[2,512]{1,0:T(2,128)S(1)}, f32[2,512]{1,0:T(2,128)S(1)}, /*index=5*/f32[2,512,128]{2,1,0:T(8,128)S(1)})) conditional(s32[]{:T(128)} %convert_element_type.94, (f32[2,512]{1,0:T(2,128)S(1)}, f32[2,512]{1,0:T(2,128)S(1)}, ...), branch_computations={%region_1.0_spmd, %region_2.6_spmd} | conditional | flops 410784768 | bytes 17705066 | solution.py:120
  247.7 5.6 %conditional.3 = ((f32[2,512]{1,0:T(2,128)S(1)}, f32[2,512]{1,0:T(2,128)S(1)}, f32[2,512,128]{2,1,0:T(8,128)S(1)}, f32[2,512]{1,0:T(2,128)S(1)}, f32[2,512]{1,0:T(2,128)S(1)}, /*index=5*/f32[2,512,128]{2,1,0:T(8,128)S(1)})) conditional(s32[]{:T(128)} %convert_element_type.94, (f32[2,512]{1,0:T(2,128)S(1)}, f32[2,512]{1,0:T(2,128)S(1)}, ...), branch_computations={%region_1.0_spmd, %region_2.6_spmd} | conditional | flops 410784768 | bytes 17705066 | solution.py:120
  253.4 5.6 %conditional.3 = ((f32[2,512]{1,0:T(2,128)S(1)}, f32[2,512]{1,0:T(2,128)S(1)}, f32[2,512,128]{2,1,0:T(8,128)S(1)}, f32[2,512]{1,0:T(2,128)S(1)}, f32[2,512]{1,0:T(2,128)S(1)}, /*index=5*/f32[2,512,128]{2,1,0:T(8,128)S(1)})) conditional(s32[]{:T(128)} %convert_element_type.94, (f32[2,512]{1,0:T(2,128)S(1)}, f32[2,512]{1,0:T(2,128)S(1)}, ...), branch_computations={%region_1.0_spmd, %region_2.6_spmd} | conditional | flops 410784768 | bytes 17705066 | solution.py:120
  264.6 5.6 %conditional.3 = ((f32[2,512]{1,0:T(2,128)S(1)}, f32[2,512]{1,0:T(2,128)S(1)}, f32[2,512,128]{2,1,0:T(8,128)S(1)}, f32[2,512]{1,0:T(2,128)S(1)}, f32[2,512]{1,0:T(2,128)S(1)}, /*index=5*/f32[2,512,128]{2,1,0:T(8,128)S(1)})) conditional(s32[]{:T(128)} %convert_element_type.94, (f32[2,512]{1,0:T(2,128)S(1)}, f32[2,512]{1,0:T(2,128)S(1)}, ...), branch_computations={%region_1.0_spmd, %region_2.6_spmd} | conditional | flops 410784768 | bytes 17705066 | solution.py:120
  270.3 5.6 %conditional.3 = ((f32[2,512]{1,0:T(2,128)S(1)}, f32[2,512]{1,0:T(2,128)S(1)}, f32[2,512,128]{2,1,0:T(8,128)S(1)}, f32[2,512]{1,0:T(2,128)S(1)}, f32[2,512]{1,0:T(2,128)S(1)}, /*index=5*/f32[2,512,128]{2,1,0:T(8,128)S(1)})) conditional(s32[]{:T(128)} %convert_element_type.94, (f32[2,512]{1,0:T(2,128)S(1)}, f32[2,512]{1,0:T(2,128)S(1)}, ...), branch_computations={%region_1.0_spmd, %region_2.6_spmd} | conditional | flops 410784768 | bytes 17705066 | solution.py:120
  282.7 9.3 %all_to_all.29 = bf16[4,128,256]{2,1,0:T(8,128)(2,1)S(1)} all-to-all(bf16[4,128,256]{2,1,0:T(8,128)(2,1)S(1)} %all_to_all.20), channel_id=1, replica_groups=mesh['sp'=32,'tp'=4] {'tp'}, dimensions={0} | all-to-all | bytes 524288 | tf_op jit(solution)/shard_map/all_to_all | solution.py:129
  300.7 23.0 %all-to-all-done.1 = bf16[4,128,2048]{2,1,0:T(8,128)(2,1)S(1)} async-done(((bf16[4,128,2048]{2,1,0:T(8,128)(2,1)}), bf16[4,128,2048]{2,1,0:T(8,128)(2,1)S(1)}, u32[]{:S(2)}, u32[]{:S(2)}) %all-to-all-start.1) | async-done | bytes 2097184 | tf_op jit(solution)/shard_map/all_to_all | solution.py:29
  323.7 9.3 %convolution_convert_fusion = bf16[512,2048]{1,0:T(8,128)(2,1)} fusion(bf16[1024,2048]{0,1:T(8,128)(2,1)} %all-gather.8.cloned.1.call-done, bf16[512,2048]{1,0:T(8,128)(2,1)S(1)} %bitcast.49, bf16[2048,1024]{1,0:T(8,128)(2,1)} %all-gather.6.cloned.1.call-done), kind=kOutput, calls=%fused_computation.29 | convolution fusion | flops 4297588736 | bytes 12582912 | tf_op jit(solution)/shard_map/dot_general | solution.py:150
  333.1 27.9 %all_to_all.30 = bf16[4,128,2048]{2,1,0:T(8,128)(2,1)S(1)} all-to-all(bf16[4,128,2048]{2,1,0:T(8,128)(2,1)} %bitcast.50), channel_id=1, replica_groups=mesh['sp'=32,'tp'=4] {'tp'}, dimensions={0} | all-to-all | bytes 4194304 | tf_op jit(solution)/shard_map/all_to_all | solution.py:46
  (593 shorter events, 230.5 us)
Async XLA Ops:
  6.5 4.6 %copy-start.1 = (bf16[512,256]{1,0:T(8,128)(2,1)S(1)}, bf16[512,256]{1,0:T(8,128)(2,1)}, u32[]{:S(2)}) copy-start(bf16[512,256]{1,0:T(8,128)(2,1)} %param.15) | copy-start | bytes 786436
  6.5 83.0 %all-gather.4.cloned.1.call-start = ((), (), s32[]{:S(2)}) async-start(), calls=%async_computation.3 | async-start | bytes 17301504 | tf_op jit(solution)/shard_map/all_gather | solution.py:14
  9.6 291.0 %all-gather.6.cloned.1.call-start = ((), (), s32[]{:S(2)}) async-start(), calls=%async_computation.4 | async-start | bytes 4325376 | tf_op jit(solution)/shard_map/all_gather | solution.py:141
  10.4 290.3 %all-gather.8.cloned.1.call-start = ((), (), s32[]{:S(2)}) async-start(), calls=%async_computation.5 | async-start | bytes 4325376 | tf_op jit(solution)/shard_map/all_gather | solution.py:142
  101.1 180.4 %copy-start.3 = (f32[2]{0:T(128)S(1)}, f32[2]{0:T(128)}, u32[]{:S(2)}) copy-start(f32[2]{0:T(128)} %param.18) | copy-start | bytes 28
  101.1 181.0 %copy-start.4 = (f32[128]{0:T(128)S(1)}, f32[128]{0:T(128)}, u32[]{:S(2)}) copy-start(f32[128]{0:T(128)} %param.19) | copy-start | bytes 1540
  281.5 10.7 %copy-start = (bf16[128,2048]{1,0:T(8,128)(2,1)S(1)}, bf16[128,2048]{1,0:T(8,128)(2,1)}, u32[]{:S(2)}) copy-start(bf16[128,2048]{1,0:T(8,128)(2,1)} %param.14) | copy-start | bytes 1572868
  292.2 3.0 copy-start.2
  297.0 26.7 %all-to-all-start.1 = ((bf16[4,128,2048]{2,1,0:T(8,128)(2,1)}), bf16[4,128,2048]{2,1,0:T(8,128)(2,1)S(1)}, u32[]{:S(2)}, u32[]{:S(2)}) async-start(bf16[4,128,2048]{2,1,0:T(8,128)(2,1)} %broadcast_in_dim.33), calls=%async_computation.1 | async-start | bytes 4194304 | tf_op jit(solution)/shard_map/all_to_all | solution.py:29
Sparse Core Ops, SparseCore 0:
  9.8 79.7 all-gather.3
  91.8 45.6 all-gather.5
  139.7 45.4 all-gather.7
where the time goes:
time: 371 us; the launch traced here: 369 us
  waiting for transfers between devices  103 us (28%)
  matrix products  97.5 us (26%)
  local copies, waits for them, and re-layouts  79 us (21%)
  blocking collectives  37.2 us (10%)
  other arithmetic  30.6 us (8%)
  between operations  13.3 us (4%)
  loops' own time  4.84 us (1%)
    all_gather x1, waiting for transfers between devices, sent_together(): whole, at, done = (lax.all_gather(both, axis, axis=dim, tiled=True), 0, [])  78.2 us
    dot_general x64, matrix products, update(): jnp.einsum('hqk,khd->hqd', exponent.astype(jnp.bfloat16), value_block, pr...  45.2 us
    dot_general x64, matrix products, update(): jnp.einsum('qhd,khd->hqk', query_split[:, :, map_index], key_block[:, :,...  39.9 us
    dynamic_slice x32, local copies, waits for them, and re-layouts, update(): lax.dynamic_slice_in_dim(value_piece, offset, block_width, 0)  31.2 us
    dynamic_slice x32, local copies, waits for them, and re-layouts, update(): lax.dynamic_slice_in_dim(key_piece, offset, block_width, 0)  31.2 us
    all_to_all x1, blocking collectives, sum_at_owner(): lax.all_to_all(cut_along(array, dim, count), axis, 0, 0, tiled=True)  27.9 us
    all_to_all x1, waiting for transfers between devices, from_everyone(): lax.all_to_all(jnp.broadcast_to(array[None], (count, *array.shape)), axis...  23 us
    reduce_sum x64, other arithmetic, update(): new_total = run_total * shrink + jnp.sum(exponent, axis=2)  19.4 us
  transfers between devices with their start and end apart: 4, of which 2 were waited for; matrix products, arithmetic and copies ran while one was open for 52% of the time, Pallas kernels for 0%

commit v1 on v0

v1 whole, which is shorter than its diff:
```python
import functools

import jax
import jax.numpy as jnp
from jax import lax
from jax.experimental import pallas as pl
from jax.experimental.pallas import tpu as pltpu
from jax.sharding import PartitionSpec as P

DQK = 64
DV = 128
BLK = 512


def attn_kernel(chip_ref, lam_ref, gain_ref, q_ref, kv_hbm, o_ref, kv_ref, s_ref, acc_ref, sems):
    chip = chip_ref[0]
    lam = lam_ref[0]
    n_a = 2 * chip + 1
    n_b = 32 - 2 * chip
    n_long = jnp.maximum(n_a, n_b)
    n_short = jnp.minimum(n_a, n_b)

    def copy_of(t):
        rows = pl.ds(pl.multiple_of(t * BLK, BLK), BLK)
        return pltpu.make_async_copy(kv_hbm.at[rows], kv_ref.at[rows], sems.at[t])

    @pl.loop(0, n_long)
    def _(t):
        copy_of(t).start()

    ones = jnp.ones((16, BLK), jnp.bfloat16)

    def run_block(b, count, waited_from):
        q1 = (q_ref[b, :, :DQK].astype(jnp.float32) * DQK ** -0.5).astype(jnp.bfloat16)
        q2 = (q_ref[b, :, DQK:].astype(jnp.float32) * DQK ** -0.5).astype(jnp.bfloat16)
        zero = jnp.zeros_like(q1)
        q_pair = (
            jnp.concatenate([q1, zero], axis=1),
            jnp.concatenate([zero, q2], axis=1),
        )

        def one_step(t, state, masked):
            @pl.when(t >= waited_from)
            def _():
                copy_of(t).wait()

            rows = pl.ds(pl.multiple_of(t * BLK, BLK), BLK)
            key = kv_ref[rows, :DV]
            val = kv_ref[rows, DV:]
            val_t = jnp.concatenate([val.T, ones], axis=0)
            out = []
            for j in range(2):
                run_max, acc = state[2 * j], state[2 * j + 1]
                scores = lax.dot_general(
                    key, q_pair[j], (((1,), (1,)), ((), ())), preferred_element_type=jnp.float32
                )
                if masked:
                    k_pos = lax.broadcasted_iota(jnp.int32, (BLK, BLK), 0)
                    q_pos = lax.broadcasted_iota(jnp.int32, (BLK, BLK), 1)
                    scores = jnp.where(k_pos <= q_pos, scores, -1e30)
                new_max = jnp.maximum(run_max, jnp.max(scores, axis=0, keepdims=True))
                shrink = jnp.exp(run_max - new_max)
                weights = jnp.exp(scores - new_max).astype(jnp.bfloat16)
                acc = acc * shrink + jnp.dot(val_t, weights, preferred_element_type=jnp.float32)
                out += [new_max, acc]
            return tuple(out)

        top = jnp.full((1, BLK), -1e30, jnp.float32)
        empty = jnp.zeros((DV + 16, BLK), jnp.float32)
        state = lax.fori_loop(
            0, count - 1, lambda t, st: one_step(t, st, False), (top, empty, top, empty)
        )
        state = one_step(count - 1, state, True)
        map_1 = state[1][:DV] / state[1][DV : DV + 1]
        map_2 = state[3][:DV] / state[3][DV : DV + 1]
        differ = map_1 - lam * map_2
        spread = lax.rsqrt(jnp.mean(differ * differ, axis=0, keepdims=True) + 1e-06)
        out = (differ * spread).T * gain_ref[...]
        o_ref[b] = out.astype(jnp.bfloat16)

    run_block(0, n_short, 0)
    run_block(1, n_long, n_short)


def attention(chip, lam, gain, q, kv):
    rows = kv.shape[0]
    smem = pl.BlockSpec(memory_space=pltpu.SMEM)
    vmem = pl.BlockSpec(memory_space=pltpu.VMEM)
    return pl.pallas_call(
        attn_kernel,
        out_shape=jax.ShapeDtypeStruct((2, BLK, DV), jnp.bfloat16),
        in_specs=[smem, smem, vmem, vmem, pl.BlockSpec(memory_space=pl.ANY)],
        out_specs=vmem,
        scratch_shapes=[
            pltpu.VMEM((rows, 2 * DV), jnp.bfloat16),
            pltpu.VMEM((BLK, BLK), jnp.float32),
            pltpu.VMEM((DV, BLK), jnp.float32),
            pltpu.SemaphoreType.DMA((rows // BLK,)),
        ],
        compiler_params=pltpu.CompilerParams(vmem_limit_bytes=48 * 1024 * 1024),
        cost_estimate=pl.CostEstimate(
            flops=24_000_000_000, bytes_accessed=16_000_000, transcendentals=17_000_000
        ),
    )(chip, lam, gain, q, kv)


def per_device(
    tokens,
    queries,
    keys,
    values,
    lambdas,
    head_gain,
    out_weight,
    mixer_gain,
    up_weight,
    down_weight,
):
    sp = lax.axis_index("sp")
    core = sp % 2
    chip = sp // 2
    count = lax.axis_size("sp")
    chips = count // 2
    first = core == 0

    def mine(a):
        return jnp.where(first, a[:, :DV], a[:, DV:])

    def other(a):
        return jnp.where(first, a[:, DV:], a[:, :DV])

    kept = jnp.concatenate([mine(keys), mine(values)], axis=1)
    sent = jnp.concatenate([other(keys), other(values)], axis=1)
    got = lax.ppermute(sent, "sp", [(s, s ^ 1) for s in range(count)])
    kv = jnp.concatenate([jnp.where(first, kept, got), jnp.where(first, got, kept)], axis=0)
    same_core = [[2 * i + c for i in range(chips)] for c in range(2)]
    kv_all = lax.all_gather(kv, "sp", axis=0, tiled=True, axis_index_groups=same_core)

    swap = []
    keep = []
    for i in range(chips):
        swap += [(2 * i, 2 * i + 1), (2 * i + 1, 2 * (chips - 1 - i))]
        keep += [(2 * i, 2 * i), (2 * i + 1, 2 * (chips - 1 - i) + 1)]
    back_swap = [(d, s) for s, d in swap]
    back_keep = [(d, s) for s, d in keep]
    q_swap = lax.ppermute(other(queries), "sp", swap)
    q_keep = lax.ppermute(mine(queries), "sp", keep)
    q_low = jnp.where(first, q_keep, q_swap)
    q_high = jnp.where(first, q_swap, q_keep)
    ordered = chip < chips // 2
    q = jnp.stack([jnp.where(ordered, q_low, q_high), jnp.where(ordered, q_high, q_low)])
    lam = jnp.where(first, lambdas[0], lambdas[1]).reshape(1)
    out = attention(chip.reshape(1), lam, head_gain.reshape(1, DV), q, kv_all)
    o_low = jnp.where(ordered, out[0], out[1])
    o_high = jnp.where(ordered, out[1], out[0])
    r_swap = lax.ppermute(jnp.where(first, o_high, o_low), "sp", back_swap)
    r_keep = lax.ppermute(jnp.where(first, o_low, o_high), "sp", back_keep)
    attended = jnp.concatenate(
        [jnp.where(first, r_keep, r_swap), jnp.where(first, r_swap, r_keep)], axis=1
    )

    tokens_all = lax.all_gather(tokens, "tp", axis=0, tiled=True)
    all_heads = lax.all_gather(attended, "tp", axis=1, tiled=True)
    projected = jnp.dot(all_heads, out_weight, preferred_element_type=jnp.float32).astype(
        jnp.bfloat16
    )
    resid = (tokens_all.astype(jnp.float32) + projected.astype(jnp.float32)).astype(jnp.bfloat16)
    resid_full = resid.astype(jnp.float32)
    normed = (
        resid_full
        * lax.rsqrt(jnp.mean(resid_full * resid_full, axis=1, keepdims=True) + 1e-06)
        * mixer_gain
    ).astype(jnp.bfloat16)
    up_full = lax.all_gather(up_weight, "sp", axis=0, tiled=True)
    down_full = lax.all_gather(down_weight, "sp", axis=1, tiled=True)
    hidden = jnp.square(
        jax.nn.relu(jnp.dot(normed, up_full, preferred_element_type=jnp.float32))
    ).astype(jnp.bfloat16)
    partial = jnp.dot(hidden, down_full, preferred_element_type=jnp.float32).astype(jnp.bfloat16)
    rows = tokens.shape[0]
    pieces = lax.all_to_all(
        partial.reshape(-1, rows, partial.shape[1]), "tp", 0, 0, tiled=True
    )
    mixed = jnp.sum(pieces.astype(jnp.float32), axis=0)
    own = lax.dynamic_slice_in_dim(resid, lax.axis_index("tp") * rows, rows, 0)
    return (own.astype(jnp.float32) + mixed).astype(jnp.bfloat16)


def solution(mesh):
    placed = (
        P(("sp", "tp"), None),
        P("sp", "tp"),
        P("sp", "tp"),
        P("sp", "tp"),
        P("tp"),
        P(),
        P(),
        P(),
        P("sp", "tp"),
        P("tp", "sp"),
    )
    return jax.shard_map(
        per_device, mesh=mesh, in_specs=placed, out_specs=P(("sp", "tp"), None), check_vma=False
    )
```

time: 371 us -> 307 us (0.83)
  the two profiles are of different devices: /device:TPU:121 before, /device:TPU:0 now
where the time goes in v1:
time: 307 us
  waiting for transfers between devices  212 us (69%)
  Pallas kernels  40.9 us (13%)
  starting transfers between devices  19.2 us (6%)
  matrix products  15.1 us (5%)
  between operations  14.5 us (5%)
  other arithmetic  5.36 us (2%)
    all_gather x1, waiting for transfers between devices, per_device(): lax.all_gather(kv, 'sp', axis=0, tiled=True, axis_index_groups=same_core)  61.1 us
    all_gather x1, waiting for transfers between devices, per_device(): down_full = lax.all_gather(down_weight, 'sp', axis=1, tiled=True)  47.6 us
    all_gather x1, waiting for transfers between devices, per_device(): up_full = lax.all_gather(up_weight, 'sp', axis=0, tiled=True)  43.6 us
    pallas_call x1, Pallas kernels, attention(): pl.pallas_call(attn_kernel, out_shape=jax.ShapeDtypeStruct((2, BLK, DV),...  40.9 us
    all_to_all x1, waiting for transfers between devices, per_device(): lax.all_to_all(partial.reshape(-1, rows, partial.shape[1]), 'tp', 0, 0, t...  26.7 us
    all_gather x1, waiting for transfers between devices, per_device(): all_heads = lax.all_gather(attended, 'tp', axis=1, tiled=True)  25.3 us
    dot_general x1, matrix products, per_device(): jnp.dot(hidden, down_full, preferred_element_type=jnp.float32)  9.39 us
    ppermute x1, starting transfers between devices, per_device(): q_swap = lax.ppermute(other(queries), 'sp', swap)  7.76 us
  transfers between devices with their start and end apart: 11, of which 8 were waited for; matrix products, arithmetic and copies ran while one was open for 2% of the time, Pallas kernels for 13%

profile of v1, /device:TPU:0, one launch (start us, length us, event | category | flops | bytes accessed | tf_op | source)
XLA Modules:
  0.0 307.2 jit_solution(16045800767800114106)
XLA Ops:
  6.5 1.2 broadcast_select_fusion.8
  7.8 0.1 collective-permute-start.2
  7.9 1.5 collective-permute-done.2
  9.4 0.1 broadcast_select_fusion.1
  9.5 0.8 pad_maximum_fusion
  10.3 0.0 all-gather.6.cloned.1.call-start
  10.4 0.7 collective-permute-start
  11.1 7.8 %collective-permute-start.1 = (bf16[512,128]{1,0:T(8,128)(2,1)S(1)}, bf16[512,128]{1,0:T(8,128)(2,1)S(1)}, u32[]{:S(2)}, u32[]{:S(2)}) collective-permute-start(bf16[512,128]{1,0:T(8,128)(2,1)S(1)} %get-tuple-element.17), channel_id=1, source_target_pairs={{0,4},{4,120},{8,12},{12,112},{16,20},{20,104},{24,28},{28,96},{32... | collective-permute-start | bytes 393224 | tf_op jit(solution)/shard_map/ppermute | solution.py:146
  18.9 0.0 all-gather.6.cloned.1.call-update
  18.9 0.0 all-gather.10.cloned.1.call-start
  19.0 0.6 fusion.12
  20.7 2.0 collective-permute-done.1
  22.8 61.1 %all-gather.8.cloned.1.call-done.kv_hbm = bf16[16384,256]{1,0:T(8,128)(2,1)} async-done(((bf16[1024,256]{1,0:T(8,128)(2,1)}), bf16[16384,256]{1,0:T(8,128)(2,1)}) %all-gather.8.cloned.1.call-update) | async-done | bytes 8388624 | tf_op jit(solution)/shard_map/all_gather | solution.py:137
  83.9 40.9 %shard_map.100 = bf16[2,512,128]{2,1,0:T(8,128)(2,1)S(1)} custom-call(s32[1]{0:T(128)} %bitcast.chip_ref, f32[1]{0:T(128)} %bitcast.3.lam_ref, f32[1,128]{1,0:T(1,128)S(1)} %bitcast.18, bf16[2,512,128]{2,1,0:T(8,128)(2,1)S(1)} %pad_maximum_fusion.1.q_ref, bf16[16384,256]{1,0:T(8,128)(2,1)} %all-gather.8.cloned.1.call-done.kv_hbm), custom_call_target="tpu_custom_call" | custom-call | flops 24000000000 | bytes 16000000 | tf_op jit(solution)/shard_map/pallas_call | solution.py:89
  124.9 0.7 collective-permute-start.3
  125.6 5.6 %collective-permute-start.4 = (bf16[512,128]{1,0:T(8,128)(2,1)S(1)}, bf16[512,128]{1,0:T(8,128)(2,1)S(1)}, u32[]{:S(2)}, u32[]{:S(2)}) collective-permute-start(bf16[512,128]{1,0:T(8,128)(2,1)S(1)} %get-tuple-element.10), channel_id=1, source_target_pairs={{4,0},{120,4},{12,8},{112,12},{20,16},{104,20},{28,24},{96,28},{36... | collective-permute-start | bytes 393224 | tf_op jit(solution)/shard_map/ppermute | solution.py:156
  131.2 2.5 collective-permute-done.4
  133.8 0.7 pad_maximum_fusion.4
  134.5 0.0 all-gather.12.cloned.1.call-start
  134.6 0.5 all-gather.12.cloned.1.call-update
  135.1 0.0 all-gather.14.cloned.1.call-start
  135.2 0.5 all-gather.14.cloned.1.call-update
  135.7 0.0 all-gather.6.cloned.1.call-done
  135.7 25.3 %all-gather.10.cloned.1.call-done = bf16[512,1024]{1,0:T(8,128)(2,1)} async-done(((bf16[512,256]{1,0:T(8,128)(2,1)}), bf16[512,1024]{1,0:T(8,128)(2,1)}) %all-gather.10.cloned.1.call-update) | async-done | bytes 1048592 | tf_op jit(solution)/shard_map/all_gather | solution.py:163
  161.1 5.7 %fusion = (f32[512]{0:T(512)S(1)}, bf16[512,2048]{1,0:T(8,128)(2,1)S(1)}) fusion(bf16[512,1024]{1,0:T(8,128)(2,1)} %all-gather.10.cloned.1.call-done, bf16[1024,2048]{1,0:T(8,128)(2,1)} %param.16, bf16[512,2048]{1,0:T(8,128)(2,1)} %all-gather.6.cloned.1.call-done), kind=kOutput, calls=%fused_computation.2 | convolution fusion | flops 2155871744 | bytes 9439232 | tf_op jit(solution)/shard_map/dot_general | solution.py:164
  166.8 43.6 %all-gather.12.cloned.1.call-done = bf16[2048,1024]{1,0:T(8,128)(2,1)} async-done(((bf16[64,1024]{1,0:T(8,128)(2,1)}), bf16[2048,1024]{1,0:T(8,128)(2,1)}) %all-gather.12.cloned.1.call-update) | async-done | bytes 4194320 | tf_op jit(solution)/shard_map/all_gather | solution.py:174
  210.4 47.6 %all-gather.14.cloned.1.call-done = bf16[1024,2048]{0,1:T(8,128)(2,1)} async-done(((bf16[1024,64]{0,1:T(8,128)(2,1)}), bf16[1024,2048]{0,1:T(8,128)(2,1)}) %all-gather.14.cloned.1.call-update) | async-done | bytes 4194320 | tf_op jit(solution)/shard_map/all_gather | solution.py:175
  258.0 9.4 %convolution_convert_fusion = bf16[512,2048]{1,0:T(8,128)(2,1)} fusion(bf16[1024,2048]{0,1:T(8,128)(2,1)} %all-gather.14.cloned.1.call-done, bf16[2048,1024]{1,0:T(8,128)(2,1)} %all-gather.12.cloned.1.call-done, bf16[512,2048]{1,0:T(8,128)(2,1)S(1)} %get-tuple-element.22, f32[2048]{0:T(1024)S(1)} %copy-done.4, f32[512]{0:T(512)S(1)} %add_rsqrt_fusion), kind=kOutput, calls=%fused_computation.7 | convolution fusion | flops 4301783040 | bytes 12593152 | tf_op jit(solution)/shard_map/dot_general | solution.py:179
  267.4 4.2 %all-to-all-start = ((bf16[4,128,2048]{2,1,0:T(8,128)(2,1)}), bf16[4,128,2048]{2,1,0:T(8,128)(2,1)S(1)}, u32[]{:S(2)}, u32[]{:S(2)}) async-start(bf16[4,128,2048]{2,1,0:T(8,128)(2,1)} %bitcast.19), calls=%async_computation | async-start | bytes 4194304 | tf_op jit(solution)/shard_map/all_to_all | solution.py:181
  271.6 26.7 %all-to-all-done = bf16[4,128,2048]{2,1,0:T(8,128)(2,1)S(1)} async-done(((bf16[4,128,2048]{2,1,0:T(8,128)(2,1)}), bf16[4,128,2048]{2,1,0:T(8,128)(2,1)S(1)}, u32[]{:S(2)}, u32[]{:S(2)}) %all-to-all-start) | async-done | bytes 2097184 | tf_op jit(solution)/shard_map/all_to_all | solution.py:181
  298.3 0.4 convert_reduce_fusion
  298.7 2.0 add_convert_fusion.1
  (22 shorter events, 0.2 us)
Async XLA Ops:
  6.5 3.9 %copy-start.1 = (bf16[512,256]{1,0:T(8,128)(2,1)S(1)}, bf16[512,256]{1,0:T(8,128)(2,1)}, u32[]{:S(2)}) copy-start(bf16[512,256]{1,0:T(8,128)(2,1)} %param.11) | copy-start | bytes 786436
  6.5 12.4 %copy-start.3 = (f32[2]{0:T(128)S(1)}, f32[2]{0:T(128)}, u32[]{:S(2)}) copy-start(f32[2]{0:T(128)} %param.14) | copy-start | bytes 28
  6.5 77.4 %copy-start = (f32[128]{0:T(128)S(1)}, f32[128]{0:T(128)}, u32[]{:S(2)}) copy-start(f32[128]{0:T(128)} %param.15) | copy-start | bytes 1540
  6.5 77.4 %all-gather.8.cloned.1.call-start = ((), (), s32[]{:S(2)}) async-start(), calls=%async_computation.2 | async-start | bytes 8912896 | tf_op jit(solution)/shard_map/all_gather | solution.py:137
  7.8 1.6 collective-permute-start.2
  10.3 125.4 %all-gather.6.cloned.1.call-start = ((), (), s32[]{:S(2)}) async-start(), calls=%async_computation.1 | async-start | bytes 2621440 | tf_op jit(solution)/shard_map/all_gather | solution.py:162
  10.4 10.3 %collective-permute-start = (bf16[512,128]{1,0:T(8,128)(2,1)S(1)}, bf16[512,128]{1,0:T(8,128)(2,1)S(1)}, u32[]{:S(2)}, u32[]{:S(2)}) collective-permute-start(bf16[512,128]{1,0:T(8,128)(2,1)S(1)} %get-tuple-element.18), channel_id=1, source_target_pairs={{0,0},{4,124},{8,8},{12,116},{16,16},{20,108},{24,24},{28,100},{32... | collective-permute-start | bytes 393224 | tf_op jit(solution)/shard_map/ppermute | solution.py:147
  11.1 11.6 %collective-permute-start.1 = (bf16[512,128]{1,0:T(8,128)(2,1)S(1)}, bf16[512,128]{1,0:T(8,128)(2,1)S(1)}, u32[]{:S(2)}, u32[]{:S(2)}) collective-permute-start(bf16[512,128]{1,0:T(8,128)(2,1)S(1)} %get-tuple-element.17), channel_id=1, source_target_pairs={{0,4},{4,120},{8,12},{12,112},{16,20},{20,104},{24,28},{28,96},{32... | collective-permute-start | bytes 393224 | tf_op jit(solution)/shard_map/ppermute | solution.py:146
  18.9 142.2 %all-gather.10.cloned.1.call-start = ((), (), s32[]{:S(2)}) async-start(), calls=%async_computation.3 | async-start | bytes 1310720 | tf_op jit(solution)/shard_map/all_gather | solution.py:163
  124.9 6.3 %collective-permute-start.3 = (bf16[512,128]{1,0:T(8,128)(2,1)S(1)}, bf16[512,128]{1,0:T(8,128)(2,1)S(1)}, u32[]{:S(2)}, u32[]{:S(2)}) collective-permute-start(bf16[512,128]{1,0:T(8,128)(2,1)S(1)} %get-tuple-element.9), channel_id=1, source_target_pairs={{0,0},{124,4},{8,8},{116,12},{16,16},{108,20},{24,24},{100,28},{32... | collective-permute-start | bytes 393224 | tf_op jit(solution)/shard_map/ppermute | solution.py:157
  125.6 8.2 %collective-permute-start.4 = (bf16[512,128]{1,0:T(8,128)(2,1)S(1)}, bf16[512,128]{1,0:T(8,128)(2,1)S(1)}, u32[]{:S(2)}, u32[]{:S(2)}) collective-permute-start(bf16[512,128]{1,0:T(8,128)(2,1)S(1)} %get-tuple-element.10), channel_id=1, source_target_pairs={{4,0},{120,4},{12,8},{112,12},{20,16},{104,20},{28,24},{96,28},{36... | collective-permute-start | bytes 393224 | tf_op jit(solution)/shard_map/ppermute | solution.py:156
  134.5 75.8 %all-gather.12.cloned.1.call-start = ((), (), s32[]{:S(2)}) async-start(), calls=%async_computation.4 | async-start | bytes 4325376 | tf_op jit(solution)/shard_map/all_gather | solution.py:174
  135.1 122.8 %all-gather.14.cloned.1.call-start = ((), (), s32[]{:S(2)}) async-start(), calls=%async_computation.5 | async-start | bytes 4325376 | tf_op jit(solution)/shard_map/all_gather | solution.py:175
  135.7 122.3 %copy-start.4 = (f32[2048]{0:T(1024)S(1)}, f32[2048]{0:T(1024)}, u32[]{:S(2)}) copy-start(f32[2048]{0:T(1024)} %param.17) | copy-start | bytes 24580
  166.8 100.6 %copy-start.2 = (bf16[512,2048]{1,0:T(8,128)(2,1)}, bf16[512,2048]{1,0:T(8,128)(2,1)S(1)}, u32[]{:S(2)}) copy-start(bf16[512,2048]{1,0:T(8,128)(2,1)S(1)} %get-tuple-element.22) | copy-start | bytes 6291460
  267.4 31.0 %all-to-all-start = ((bf16[4,128,2048]{2,1,0:T(8,128)(2,1)}), bf16[4,128,2048]{2,1,0:T(8,128)(2,1)S(1)}, u32[]{:S(2)}, u32[]{:S(2)}) async-start(bf16[4,128,2048]{2,1,0:T(8,128)(2,1)} %bitcast.19), calls=%async_computation | async-start | bytes 4194304 | tf_op jit(solution)/shard_map/all_to_all | solution.py:181
Sparse Core Ops, SparseCore 0:
  10.5 73.4 all-gather.7
  85.6 30.2 all-gather.5
  134.7 26.3 all-gather.9
  163.2 47.1 all-gather.11
  212.5 45.4 all-gather.13

commit v2 on v0

v2 whole, which is shorter than its diff:
```python
import jax
import jax.numpy as jnp
from jax import lax
from jax.experimental import pallas as pl
from jax.experimental.pallas import tpu as pltpu
from jax.sharding import PartitionSpec as P

MESH = pl.DeviceIdType.MESH
DQK = 64
DV = 128
BLK = 512
HALF = 256
RING = 4
CHIPS = 16
TP = 4
D = 2048
FFT = 1024
ROWS = 128
SUMROWS = 16

HERE, LEFT, RIGHT, FAR = 0, 1, 2, 3
FIRST = (HERE, LEFT, RIGHT, HERE, HERE, FAR, HERE, LEFT, LEFT, RIGHT, RIGHT, LEFT, RIGHT, FAR, FAR, FAR)
SECOND = (HERE, HERE, HERE, LEFT, RIGHT, HERE, FAR, LEFT, RIGHT, LEFT, RIGHT, FAR, FAR, LEFT, RIGHT, FAR)


def pick(index, table):
    value = jnp.int32(0)
    for at, entry in enumerate(table):
        if entry:
            value = value + jnp.where(index == at, entry, 0)
    return value


def shift(place):
    return jnp.where(place == LEFT, 3, jnp.where(place == RIGHT, 1, jnp.where(place == FAR, 2, 0)))


def remote(src, dst, send_sem, recv_sem, sp, tp):
    return pltpu.make_async_remote_copy(
        src_ref=src,
        dst_ref=dst,
        send_sem=send_sem,
        recv_sem=recv_sem,
        device_id=(sp, tp),
        device_id_type=MESH,
    )


def layer_kernel(
    tokens,
    queries,
    keys,
    values,
    lambdas,
    head_gain,
    out_weight,
    mixer_gain,
    up_weight,
    down_weight,
    result,
    kv,
    q_in,
    q_t,
    v_t,
    run_max,
    acc,
    weights,
    out_w,
    tok,
    stage,
    att,
    resid,
    normed,
    part,
    relay,
    arrived,
    own_sem,
    load_sem,
    swap_sem,
    q_sem,
    kv_send,
    kv_recv,
    w_send,
    w_recv,
    pair_send,
    pair_recv,
    tok_send,
    tok_recv,
    back_send,
    back_recv,
    att_send,
    att_recv,
    sum_send,
    sum_recv,
):
    sp = lax.axis_index("sp")
    x = lax.axis_index("tp")
    core = lax.rem(sp, 2)
    chip = sp // 2
    y = lax.rem(chip, RING)
    z = chip // RING
    mirror = CHIPS - 1 - chip
    pair = chip * 2 + (1 - core)

    def ring(place, step):
        return lax.rem(place + step, RING)

    def at(yy, zz):
        return (zz * RING + yy) * 2 + core

    y_up, y_down = at(ring(y, 1), z), at(ring(y, 3), z)
    z_up, z_down = at(y, ring(z, 1)), at(y, ring(z, 3))
    x_up, x_down = ring(x, 1), ring(x, 3)

    barrier = pltpu.get_barrier_semaphore()
    greeted = [(s, x) for s in (y_up, y_down, z_up, z_down, pair, mirror * 2, mirror * 2 + 1)]
    greeted += [(sp, x_up), (sp, x_down)]
    for device in greeted:
        pl.semaphore_signal(barrier, inc=1, device_id=device, device_id_type=MESH)
    pl.semaphore_wait(barrier, len(greeted))

    def lanes(place):
        return pl.ds(pl.multiple_of(place * DV, DV), DV)

    mine = lanes(core)
    theirs = lanes(1 - core)
    own_q = pltpu.make_async_copy(queries.at[:, pl.ds(0, DV)], q_in.at[0], own_sem.at[0])

    def q_copy(head, slot, to):
        return remote(
            queries.at[:, pl.ds(head * DV, DV)], q_in.at[slot], q_sem.at[2 + head], q_sem.at[slot], to, x
        )

    @pl.when(core == 0)
    def _():
        q_copy(1, 0, pair).start()
        own_q.start()

    @pl.when(core == 1)
    def _():
        q_copy(0, 1, mirror * 2).start()
        q_copy(1, 1, mirror * 2 + 1).start()

    own_block = pl.ds((chip * 2 + core) * 2, 2)
    pair_block = pl.ds((chip * 2 + 1 - core) * 2, 2)
    swaps = []
    owns = []
    for number, (array, half) in enumerate(((keys, pl.ds(0, DV)), (values, pl.ds(DV, DV)))):
        for unit in range(2):
            rows = pl.ds(unit * HALF, HALF)
            place = kv.at[(chip * 2 + core) * 2 + unit, :, half]
            index = number * 2 + unit
            swaps.append(
                remote(array.at[rows, theirs], place, swap_sem.at[4 + index], swap_sem.at[index], pair, x)
            )
            owns.append(pltpu.make_async_copy(array.at[rows, mine], place, own_sem.at[1 + index]))
    for copy in swaps + owns:
        copy.start()

    own_tok = pltpu.make_async_copy(tokens, tok.at[x], own_sem.at[5])
    own_tok.start()

    def tok_copy(source, unit, to, fwd):
        rows = pl.ds(unit * (ROWS // 2), ROWS // 2)
        return remote(
            tok.at[source, rows], tok.at[source, rows], tok_send.at[fwd], tok_recv.at[source, unit], sp, to
        )

    own_w = []
    w_row = chip * 128 + core * 64
    for number, array in enumerate((up_weight, down_weight)):
        own_w.append(
            pltpu.make_async_copy(
                array, weights.at[number, pl.ds(pl.multiple_of(w_row, 64), 64)], own_sem.at[6 + number]
            )
        )
        own_w[-1].start()
    load_w = pltpu.make_async_copy(out_weight, out_w, load_sem.at[0])
    load_w.start()

    run_max[...] = jnp.full(run_max.shape, -1e30, jnp.float32)
    acc[...] = jnp.zeros(acc.shape, jnp.float32)
    v_t[DV:, :] = jnp.ones((SUMROWS, BLK), jnp.bfloat16)

    own_tok.wait()
    for unit in range(2):
        for number, to in enumerate((x_up, x_down)):
            tok_copy(x, unit, to, unit * 2 + number).start()

    for copy in owns:
        copy.wait()
    for copy in swaps:
        copy.wait_recv()

    @pl.when(core == 0)
    def _():
        own_q.wait()

    @pl.when(core == 1)
    def _():
        q_copy(0, 0, pair).wait_recv()

    q_copy(0, 1, mirror * 2).wait_recv()

    for slot in range(2):
        q_slot = (q_in[slot].astype(jnp.float32) * DQK ** -0.5).T.astype(jnp.bfloat16)
        zero = jnp.zeros((DQK, BLK), jnp.bfloat16)
        q_t[slot, 0, :DQK] = q_slot[:DQK]
        q_t[slot, 0, DQK:] = zero
        q_t[slot, 1, :DQK] = zero
        q_t[slot, 1, DQK:] = q_slot[DQK:]

    def gather_event(number, unit_ref, send_sem, recv_ref):
        odd = lax.rem(number, 2)
        first = pick(number // 2, FIRST)
        second = pick(number // 2, SECOND)
        y_step = jnp.where(odd == 0, shift(first), shift(second))
        z_step = jnp.where(odd == 0, shift(second), shift(first))
        source = ring(z, z_step) * RING + ring(y, y_step)
        first_up = jnp.where(odd == 0, y_up, z_up)
        first_down = jnp.where(odd == 0, y_down, z_down)
        second_up = jnp.where(odd == 0, z_up, y_up)
        second_down = jnp.where(odd == 0, z_down, y_down)

        def copy(unit, to):
            ref = unit_ref(odd, source, unit)
            return remote(ref, ref, send_sem, recv_ref(odd, source, unit), to, x)

        @pl.when(number >= 2)
        def _():
            for unit in range(2):
                copy(unit, sp).wait_recv()

        for unit in range(2):
            along = LEFT if unit == 0 else RIGHT
            on_first = (second == HERE) & ((first == HERE) | (first == along))
            at_start = (second == HERE) & (first == HERE)
            on_second = (second == HERE) | (second == along)
            at_turn = second == HERE
            for to, sends in (
                (first_up, on_first if unit == 0 else at_start),
                (first_down, at_start if unit == 0 else on_first),
                (second_up, on_second if unit == 0 else at_turn),
                (second_down, at_turn if unit == 0 else on_second),
            ):

                @pl.when(sends)
                def _(unit=unit, to=to):
                    copy(unit, to).start()

        return odd, source

    def kv_unit(odd, source, unit):
        return kv.at[(source * 2 + odd) * 2 + unit]

    def kv_sem(odd, source, unit):
        return kv_recv.at[(source * 2 + odd) * 2 + unit]

    def kv_body(number, carry):
        odd, source = gather_event(number, kv_unit, kv_send.at[0], kv_sem)
        block = source * 2 + odd

        @pl.when(number == 10)
        def _():
            for unit in range(2):
                tok_copy(x_down, unit, x_up, 0).wait_recv()
                tok_copy(x_up, unit, x_down, 0).wait_recv()
            tok_copy(x_down, 0, x_up, 4).start()
            tok_copy(x_up, 1, x_down, 5).start()

        key = kv[pl.ds(block * 2, 2), :, :DV].reshape(BLK, DV)
        v_t[:DV, :] = kv[pl.ds(block * 2, 2), :, DV:].reshape(BLK, DV).T

        def step(slot, masked):
            for j in range(2):
                scores = jnp.dot(key, q_t[slot, j], preferred_element_type=jnp.float32)
                if masked:
                    k_pos = lax.broadcasted_iota(jnp.int32, (BLK, BLK), 0)
                    q_pos = lax.broadcasted_iota(jnp.int32, (BLK, BLK), 1)
                    scores = jnp.where(k_pos <= q_pos, scores, -1e30)
                old_max = run_max[slot, j]
                new_max = jnp.maximum(old_max, jnp.max(scores, axis=0, keepdims=True))
                shrink = jnp.exp(old_max - new_max)
                weight = jnp.exp(scores - new_max).astype(jnp.bfloat16)
                acc[slot, j] = acc[slot, j] * shrink + jnp.dot(
                    v_t[...], weight, preferred_element_type=jnp.float32
                )
                run_max[slot, j] = new_max

        def slot_body(slot, inner):
            q_block = jnp.where(slot == 0, chip * 2, 31 - chip * 2)

            @pl.when(block < q_block)
            def _():
                step(slot, False)

            @pl.when(block == q_block)
            def _():
                step(slot, True)

            return inner

        lax.fori_loop(0, 2, slot_body, 0)
        return carry

    lax.fori_loop(0, 2 * CHIPS, kv_body, 0)

    def w_unit(odd, source, unit):
        return weights.at[odd, pl.ds(pl.multiple_of(source * 128 + core * 64 + unit * 32, 32), 32)]

    def w_sem(odd, source, unit):
        return w_recv.at[odd, source * 2 + unit]

    def w_body(number, carry):
        odd, source = gather_event(number, w_unit, w_send.at[0], w_sem)
        item = weights.at[odd, pl.ds(pl.multiple_of(source * 128 + core * 64, 64), 64)]
        remote(item, item, pair_send.at[0], pair_recv.at[0], pair, x).start()
        return carry

    for copy in own_w:
        copy.wait()
    lax.fori_loop(0, 2, w_body, 0)

    for slot in range(2):
        map_1 = acc[slot, 0, :DV] / acc[slot, 0, DV : DV + 1]
        map_2 = acc[slot, 1, :DV] / acc[slot, 1, DV : DV + 1]
        lam = jnp.where(core == 0, lambdas[0], lambdas[1])
        differ = map_1 - lam * map_2
        spread = lax.rsqrt(jnp.mean(differ * differ, axis=0, keepdims=True) + 1e-06)
        stage[slot] = ((differ * spread).T * head_gain[...]).astype(jnp.bfloat16)

    def att_lanes(head):
        return pl.ds(pl.multiple_of((x * 2 + head) * DV, DV), DV)

    def back_copy(slot, head, to):
        return remote(
            stage.at[slot], att.at[:, att_lanes(head)], back_send.at[slot], back_recv.at[head], to, x
        )

    @pl.when(core == 0)
    def _():
        att[:, att_lanes(0)] = stage[0]

    @pl.when(core == 1)
    def _():
        back_copy(0, 1, pair).start()

    back_copy(1, core, mirror * 2 + 1).start()

    lax.fori_loop(2, 10, w_body, 0)

    @pl.when(core == 1)
    def _():
        back_copy(0, 0, pair).wait_recv()

    back_copy(0, 1, pair).wait_recv()

    def att_copy(source, unit, to, sem):
        place = att.at[
            pl.ds(unit * HALF, HALF), pl.ds(pl.multiple_of(source * 2 * DV, 2 * DV), 2 * DV)
        ]
        return remote(place, place, att_send.at[sem], att_recv.at[source, unit], sp, to)

    for unit in range(2):
        for number, to in enumerate((x_up, x_down)):
            att_copy(x, unit, to, unit * 2 + number).start()

    lax.fori_loop(10, 20, w_body, 0)

    for unit in range(2):
        att_copy(x_down, unit, x_up, 0).wait_recv()
        att_copy(x_up, unit, x_down, 0).wait_recv()
    att_copy(x_down, 0, x_up, 4).start()
    att_copy(x_up, 1, x_down, 5).start()

    lax.fori_loop(20, 2 * CHIPS, w_body, 0)

    x_far = ring(x, 2)
    load_w.wait()
    for unit in range(2):
        tok_copy(x_far, unit, x_up, 0).wait_recv()
    for unit in range(2):
        att_copy(x_far, unit, x_up, 0).wait_recv()

    @pl.loop(0, 4)
    def _(column):
        cols = pl.ds(pl.multiple_of(column * 512, 512), 512)
        projected = jnp.dot(att[...], out_w[:, cols], preferred_element_type=jnp.float32).astype(
            jnp.bfloat16
        )
        tok_cols = tok[:, :, cols].reshape(BLK, 512)
        resid[:, cols] = (tok_cols.astype(jnp.float32) + projected.astype(jnp.float32)).astype(
            jnp.bfloat16
        )

    @pl.loop(0, 8)
    def _(tile):
        rows = pl.ds(pl.multiple_of(tile * 64, 64), 64)
        full = resid[rows].astype(jnp.float32)
        scale = lax.rsqrt(jnp.mean(full * full, axis=1, keepdims=True) + 1e-06)
        normed[rows] = (full * scale * mixer_gain[...]).astype(jnp.bfloat16)

    remote(weights.at[0], weights.at[0], pair_send.at[0], pair_recv.at[0], pair, x).wait_recv()

    def hidden_of(owner):
        rows = pl.ds(pl.multiple_of(owner * ROWS, ROWS), ROWS)
        hidden = jnp.dot(normed[rows], weights[0], preferred_element_type=jnp.float32)
        return jnp.square(jnp.maximum(hidden, 0.0)).astype(jnp.bfloat16)

    def down(hidden, column, width):
        return lax.dot_general(
            hidden,
            weights[1, column : column + width],
            (((1,), (1,)), ((), ())),
            preferred_element_type=jnp.float32,
        )

    wide = D // 2

    def relay_copy(number, to):
        return remote(
            part.at[0, number], relay.at[number], sum_send.at[number], sum_recv.at[number], sp, to
        )

    def final_copy(number, half, to):
        return remote(
            part.at[1 + number, half],
            arrived.at[number, half],
            sum_send.at[2 + number * 2 + half],
            sum_recv.at[2 + number * 2 + half],
            sp,
            to,
        )

    hidden = hidden_of(x_far)
    for half, to in ((0, x_up), (1, x_down)):
        part[0, half] = down(hidden, half * wide, wide).astype(jnp.bfloat16)
        relay_copy(half, to).start()

    for number, to in ((0, x_up), (1, x_down)):
        hidden = hidden_of(to)
        plain = 1 - number
        part[1 + number, plain] = down(hidden, plain * wide, wide).astype(jnp.bfloat16)
        final_copy(number, plain, to).start()
        added = down(hidden, number * wide, wide)
        relay_copy(number, to).wait_recv()
        part[1 + number, number] = (added + relay[number].astype(jnp.float32)).astype(jnp.bfloat16)
        final_copy(number, number, to).start()

    hidden = hidden_of(x)
    own_rows = pl.ds(pl.multiple_of(x * ROWS, ROWS), ROWS)
    for half in range(2):
        cols = slice(half * wide, (half + 1) * wide)
        total = down(hidden, half * wide, wide) + resid[own_rows, cols].astype(jnp.float32)
        for number in range(2):
            final_copy(number, half, x_up).wait_recv()
            total = total + arrived[number, half].astype(jnp.float32)
        result[:, cols] = total.astype(jnp.bfloat16)

    @pl.when(core == 0)
    def _():
        q_copy(1, 0, pair).wait_send()

    @pl.when(core == 1)
    def _():
        q_copy(0, 1, mirror * 2).wait_send()
        q_copy(1, 1, mirror * 2 + 1).wait_send()
        back_copy(0, 1, pair).wait_send()

    for copy in swaps:
        copy.wait_send()
    for sem in range(6):
        tok_copy(x, 0, x_up, sem).wait_send()
        att_copy(x, 0, x_up, sem).wait_send()
    sent_kv = kv.at[pl.ds(0, 60)]
    remote(sent_kv, sent_kv, kv_send.at[0], kv_recv.at[0], y_up, x).wait_send()
    sent_w = weights.at[0, pl.ds(0, 60 * 32)]
    remote(sent_w, sent_w, w_send.at[0], w_recv.at[0, 0], y_up, x).wait_send()
    remote(weights.at[0], weights.at[0], pair_send.at[0], pair_recv.at[0], pair, x).wait_send()
    back_copy(1, core, mirror * 2 + 1).wait_send()
    for number in range(2):
        relay_copy(number, x_up).wait_send()
        for half in range(2):
            final_copy(number, half, x_up).wait_send()


def per_device(
    tokens,
    queries,
    keys,
    values,
    lambdas,
    head_gain,
    out_weight,
    mixer_gain,
    up_weight,
    down_weight,
):
    any_ref = pl.BlockSpec(memory_space=pl.ANY)
    vmem = pl.BlockSpec(memory_space=pltpu.VMEM)
    smem = pl.BlockSpec(memory_space=pltpu.SMEM)
    bf16, f32 = jnp.bfloat16, jnp.float32
    dma = pltpu.SemaphoreType.DMA
    return pl.pallas_call(
        layer_kernel,
        out_shape=jax.ShapeDtypeStruct(tokens.shape, bf16),
        in_specs=[any_ref] * 4 + [smem, vmem, any_ref, vmem, any_ref, any_ref],
        out_specs=vmem,
        scratch_shapes=[
            pltpu.VMEM((64, HALF, 2 * DV), bf16),
            pltpu.VMEM((2, BLK, DV), bf16),
            pltpu.VMEM((2, 2, DV, BLK), bf16),
            pltpu.VMEM((DV + SUMROWS, BLK), bf16),
            pltpu.VMEM((2, 2, 1, BLK), f32),
            pltpu.VMEM((2, 2, DV + SUMROWS, BLK), f32),
            pltpu.VMEM((2, D, FFT), bf16),
            pltpu.VMEM((1024, D), bf16),
            pltpu.VMEM((TP, ROWS, D), bf16),
            pltpu.VMEM((2, BLK, DV), bf16),
            pltpu.VMEM((BLK, 1024), bf16),
            pltpu.VMEM((BLK, D), bf16),
            pltpu.VMEM((BLK, D), bf16),
            pltpu.VMEM((3, 2, ROWS, D // 2), bf16),
            pltpu.VMEM((2, ROWS, D // 2), bf16),
            pltpu.VMEM((2, 2, ROWS, D // 2), bf16),
            dma((8,)),
            dma((1,)),
            dma((8,)),
            dma((4,)),
            dma((1,)),
            dma((64,)),
            dma((1,)),
            dma((2, 32)),
            dma((1,)),
            dma((1,)),
            dma((6,)),
            dma((TP, 2)),
            dma((2,)),
            dma((2,)),
            dma((6,)),
            dma((TP, 2)),
            dma((6,)),
            dma((6,)),
        ],
        compiler_params=pltpu.CompilerParams(
            collective_id=0, has_side_effects=True, vmem_limit_bytes=56 * 1024 * 1024
        ),
    )(
        tokens,
        queries,
        keys,
        values,
        lambdas,
        head_gain.reshape(1, -1),
        out_weight,
        mixer_gain.reshape(1, -1),
        up_weight,
        down_weight.T,
    )


def solution(mesh):
    placed = (
        P(("sp", "tp"), None),
        P("sp", "tp"),
        P("sp", "tp"),
        P("sp", "tp"),
        P("tp"),
        P(),
        P(),
        P(),
        P("sp", "tp"),
        P("tp", "sp"),
    )
    return jax.shard_map(
        per_device, mesh=mesh, in_specs=placed, out_specs=P(("sp", "tp"), None), check_vma=False
    )
```

time: 371 us -> 138 us (0.37)
  the two profiles are of different devices: /device:TPU:121 before, /device:TPU:0 now
where the time goes in v2:
time: 138 us; the launch traced here: 137 us
  Pallas kernels  135 us (98%)
  local copies, waits for them, and re-layouts  1.88 us (1%)
    pallas_call x1, Pallas kernels, per_device(): pl.pallas_call(layer_kernel, out_shape=jax.ShapeDtypeStruct(tokens.shape,...  135 us

profile of v2, /device:TPU:0, one launch (start us, length us, event | category | flops | bytes accessed | tf_op | source)
XLA Modules:
  0.0 137.4 jit_solution(14460900579162414333)
XLA Ops:
  0.0 135.5 %shard_map.100 = bf16[128,2048]{1,0:T(8,128)(2,1)} custom-call(bf16[128,2048]{1,0:T(8,128)(2,1)} %tokens.1, bf16[512,256]{1,0:T(8,128)(2,1)} %queries.1, bf16[512,256]{1,0:T(8,128)(2,1)} %keys.1, bf16[512,256]{1,0:T(8,128)(2,1)} %values.1, f32[2]{0:T(128)} %lambdas.1, f32[1,128]{1,0:T(1,128)} %bitcast.5, bf16[1024,2048]{1,0:T(8,128)(2,1)} %out_weight.1, ...), custom_call_target="tpu_custom_call" | custom-call | tf_op jit(solution)/shard_map/pallas_call | solution.py:504
  135.5 1.9 %copy.12 = bf16[128,2048]{1,0:T(8,128)(2,1)} copy(bf16[128,2048]{1,0:T(8,128)(2,1)} %shard_map.100) | data formatting | bytes 1048576

commit v3 on v2

--- a/solution.py
+++ b/solution.py
@@ -17,6 +17,7 @@
 FFT = 1024
 ROWS = 128
 SUMROWS = 16
+W_FROM = 26
 
 HERE, LEFT, RIGHT, FAR = 0, 1, 2, 3
 FIRST = (HERE, LEFT, RIGHT, HERE, HERE, FAR, HERE, LEFT, LEFT, RIGHT, RIGHT, LEFT, RIGHT, FAR, FAR, FAR)
@@ -62,6 +63,9 @@
     q_in,
     q_t,
     v_t,
+    scores_a,
+    scores_b,
+    top,
     run_max,
     acc,
     weights,
@@ -180,7 +184,9 @@
 
     run_max[...] = jnp.full(run_max.shape, -1e30, jnp.float32)
     acc[...] = jnp.zeros(acc.shape, jnp.float32)
-    v_t[DV:, :] = jnp.ones((SUMROWS, BLK), jnp.bfloat16)
+    v_t[...] = jnp.ones(v_t.shape, jnp.bfloat16)
+    scores_b[...] = jnp.full(scores_b.shape, -1e30, jnp.float32)
+    top[...] = jnp.full(top.shape, -1e30, jnp.float32)
 
     own_tok.wait()
     for unit in range(2):
@@ -191,6 +197,66 @@
         copy.wait()
     for copy in swaps:
         copy.wait_recv()
+
+    def item_of(number):
+        odd = lax.rem(number, 2)
+        first = pick(number // 2, FIRST)
+        second = pick(number // 2, SECOND)
+        y_step = jnp.where(odd == 0, shift(first), shift(second))
+        z_step = jnp.where(odd == 0, shift(second), shift(first))
+        source = ring(z, z_step) * RING + ring(y, y_step)
+        return odd, first, second, source
+
+    def pass_on(number, ref_of, send_sem, recv_of):
+        odd, first, second, source = item_of(number)
+        first_up = jnp.where(odd == 0, y_up, z_up)
+        first_down = jnp.where(odd == 0, y_down, z_down)
+        second_up = jnp.where(odd == 0, z_up, y_up)
+        second_down = jnp.where(odd == 0, z_down, y_down)
+        at_turn = second == HERE
+        at_start = at_turn & (first == HERE)
+        halves = (second == FAR) | (at_turn & (first == FAR))
+
+        def copy(unit, to):
+            ref = ref_of(odd, source, unit)
+            return remote(ref, ref, send_sem, recv_of(odd, source, 0 if unit is None else unit), to, x)
+
+        @pl.when(jnp.logical_not(at_start) & halves)
+        def _():
+            copy(0, sp).wait_recv()
+            copy(1, sp).wait_recv()
+
+        @pl.when(jnp.logical_not(at_start | halves))
+        def _():
+            copy(None, sp).wait_recv()
+
+        for unit, to, sends in (
+            (None, first_up, at_start),
+            (None, first_down, at_start),
+            (0, first_up, at_turn & (first == LEFT)),
+            (1, first_down, at_turn & (first == RIGHT)),
+            (None, second_up, at_turn),
+            (None, second_down, at_turn),
+            (0, second_up, second == LEFT),
+            (1, second_down, second == RIGHT),
+        ):
+
+            @pl.when(sends)
+            def _(unit=unit, to=to):
+                copy(unit, to).start()
+
+    def kv_ref(odd, source, unit):
+        first = (source * 2 + odd) * 2
+        return kv.at[pl.ds(first, 2)] if unit is None else kv.at[first + unit]
+
+    def kv_sem(odd, source, unit):
+        return kv_recv.at[(source * 2 + odd) * 2 + unit]
+
+    def kv_pass(number, carry):
+        pass_on(number, kv_ref, kv_send.at[0], kv_sem)
+        return carry
+
+    lax.fori_loop(0, 2, kv_pass, 0)
 
     @pl.when(core == 0)
     def _():
@@ -210,55 +276,59 @@
         q_t[slot, 1, :DQK] = zero
         q_t[slot, 1, DQK:] = q_slot[DQK:]
 
-    def gather_event(number, unit_ref, send_sem, recv_ref):
-        odd = lax.rem(number, 2)
-        first = pick(number // 2, FIRST)
-        second = pick(number // 2, SECOND)
-        y_step = jnp.where(odd == 0, shift(first), shift(second))
-        z_step = jnp.where(odd == 0, shift(second), shift(first))
-        source = ring(z, z_step) * RING + ring(y, y_step)
-        first_up = jnp.where(odd == 0, y_up, z_up)
-        first_down = jnp.where(odd == 0, y_down, z_down)
-        second_up = jnp.where(odd == 0, z_up, y_up)
-        second_down = jnp.where(odd == 0, z_down, y_down)
-
-        def copy(unit, to):
-            ref = unit_ref(odd, source, unit)
-            return remote(ref, ref, send_sem, recv_ref(odd, source, unit), to, x)
-
+    def w_ref(odd, source, unit):
+        row = source * 128 + core * 64
+        if unit is None:
+            return weights.at[odd, pl.ds(pl.multiple_of(row, 64), 64)]
+        return weights.at[odd, pl.ds(pl.multiple_of(row + unit * 32, 32), 32)]
+
+    def w_sem(odd, source, unit):
+        return w_recv.at[odd, source * 2 + unit]
+
+    def w_pass(number, carry):
+        pass_on(number, w_ref, w_send.at[0], w_sem)
+        odd, _, _, source = item_of(number)
+        item = w_ref(odd, source, None)
+        remote(item, item, pair_send.at[0], pair_recv.at[0], pair, x).start()
+        return carry
+
+    scores_of = (scores_a, scores_b)
+
+    def absorb(before, j, weight, new_max, slot):
+        shrink = jnp.exp(run_max[slot, j] - new_max)
+        acc[slot, j] = acc[slot, j] * shrink + jnp.dot(
+            v_t[before], weight, preferred_element_type=jnp.float32
+        )
+        run_max[slot, j] = new_max
+
+    def softmax(before, j, slot):
+        new_max = jnp.maximum(run_max[slot, j], top[before, j])
+        weight = jnp.exp(scores_of[before][j] - new_max).astype(jnp.bfloat16)
+        return weight, new_max
+
+    def step(now, block, slot, last_slot, masked):
+        before = 1 - now
+        key = kv[pl.ds(block * 2, 2), :, :DV].reshape(BLK, DV)
+        v_t[now, :DV, :] = kv[pl.ds(block * 2, 2), :, DV:].reshape(BLK, DV).T
+        for j in range(2):
+            scores = jnp.dot(key, q_t[slot, j], preferred_element_type=jnp.float32)
+            if masked:
+                k_pos = lax.broadcasted_iota(jnp.int32, (BLK, BLK), 0)
+                q_pos = lax.broadcasted_iota(jnp.int32, (BLK, BLK), 1)
+                scores = jnp.where(k_pos <= q_pos, scores, -1e30)
+            scores_of[now][j] = scores
+            top[now, j] = jnp.max(scores, axis=0, keepdims=True)
+            weight, new_max = softmax(before, j, last_slot)
+            absorb(before, j, weight, new_max, last_slot)
+
+    def kv_body(number, carry):
         @pl.when(number >= 2)
         def _():
-            for unit in range(2):
-                copy(unit, sp).wait_recv()
-
-        for unit in range(2):
-            along = LEFT if unit == 0 else RIGHT
-            on_first = (second == HERE) & ((first == HERE) | (first == along))
-            at_start = (second == HERE) & (first == HERE)
-            on_second = (second == HERE) | (second == along)
-            at_turn = second == HERE
-            for to, sends in (
-                (first_up, on_first if unit == 0 else at_start),
-                (first_down, at_start if unit == 0 else on_first),
-                (second_up, on_second if unit == 0 else at_turn),
-                (second_down, at_turn if unit == 0 else on_second),
-            ):
-
-                @pl.when(sends)
-                def _(unit=unit, to=to):
-                    copy(unit, to).start()
-
-        return odd, source
-
-    def kv_unit(odd, source, unit):
-        return kv.at[(source * 2 + odd) * 2 + unit]
-
-    def kv_sem(odd, source, unit):
-        return kv_recv.at[(source * 2 + odd) * 2 + unit]
-
-    def kv_body(number, carry):
-        odd, source = gather_event(number, kv_unit, kv_send.at[0], kv_sem)
-        block = source * 2 + odd
+            kv_pass(number, 0)
+
+        @pl.when(number >= W_FROM)
+        def _():
+            w_pass(number - W_FROM, 0)
 
         @pl.when(number == 10)
         def _():
@@ -268,58 +338,31 @@
             tok_copy(x_down, 0, x_up, 4).start()
             tok_copy(x_up, 1, x_down, 5).start()
 
-        key = kv[pl.ds(block * 2, 2), :, :DV].reshape(BLK, DV)
-        v_t[:DV, :] = kv[pl.ds(block * 2, 2), :, DV:].reshape(BLK, DV).T
-
-        def step(slot, masked):
-            for j in range(2):
-                scores = jnp.dot(key, q_t[slot, j], preferred_element_type=jnp.float32)
-                if masked:
-                    k_pos = lax.broadcasted_iota(jnp.int32, (BLK, BLK), 0)
-                    q_pos = lax.broadcasted_iota(jnp.int32, (BLK, BLK), 1)
-                    scores = jnp.where(k_pos <= q_pos, scores, -1e30)
-                old_max = run_max[slot, j]
-                new_max = jnp.maximum(old_max, jnp.max(scores, axis=0, keepdims=True))
-                shrink = jnp.exp(old_max - new_max)
-                weight = jnp.exp(scores - new_max).astype(jnp.bfloat16)
-                acc[slot, j] = acc[slot, j] * shrink + jnp.dot(
-                    v_t[...], weight, preferred_element_type=jnp.float32
-                )
-                run_max[slot, j] = new_max
+        odd, _, _, source = item_of(number)
+        block = source * 2 + odd
 
         def slot_body(slot, inner):
+            now, last_slot = inner
             q_block = jnp.where(slot == 0, chip * 2, 31 - chip * 2)
-
-            @pl.when(block < q_block)
-            def _():
-                step(slot, False)
-
-            @pl.when(block == q_block)
-            def _():
-                step(slot, True)
-
-            return inner
-
-        lax.fori_loop(0, 2, slot_body, 0)
-        return carry
-
-    lax.fori_loop(0, 2 * CHIPS, kv_body, 0)
-
-    def w_unit(odd, source, unit):
-        return weights.at[odd, pl.ds(pl.multiple_of(source * 128 + core * 64 + unit * 32, 32), 32)]
-
-    def w_sem(odd, source, unit):
-        return w_recv.at[odd, source * 2 + unit]
-
-    def w_body(number, carry):
-        odd, source = gather_event(number, w_unit, w_send.at[0], w_sem)
-        item = weights.at[odd, pl.ds(pl.multiple_of(source * 128 + core * 64, 64), 64)]
-        remote(item, item, pair_send.at[0], pair_recv.at[0], pair, x).start()
-        return carry
+            for parity in range(2):
+                for masked in (False, True):
+                    wanted = (block == q_block) if masked else (block < q_block)
+
+                    @pl.when((now == parity) & wanted)
+                    def _(parity=parity, masked=masked):
+                        step(parity, block, slot, last_slot, masked)
+
+            done = block <= q_block
+            return jnp.where(done, 1 - now, now), jnp.where(done, slot, last_slot)
+
+        return lax.fori_loop(0, 2, slot_body, carry)
 
     for copy in own_w:
         copy.wait()
-    lax.fori_loop(0, 2, w_body, 0)
+    _, last_slot = lax.fori_loop(0, 2 * CHIPS, kv_body, (jnp.int32(0), jnp.int32(0)))
+    for j in range(2):
+        weight, new_max = softmax(0, j, last_slot)
+        absorb(0, j, weight, new_max, last_slot)
 
     for slot in range(2):
         map_1 = acc[slot, 0, :DV] / acc[slot, 0, DV : DV + 1]
@@ -347,7 +390,7 @@
 
     back_copy(1, core, mirror * 2 + 1).start()
 
-    lax.fori_loop(2, 10, w_body, 0)
+    lax.fori_loop(2 * CHIPS - W_FROM, 12, w_pass, 0)
 
     @pl.when(core == 1)
     def _():
@@ -365,7 +408,7 @@
         for number, to in enumerate((x_up, x_down)):
             att_copy(x, unit, to, unit * 2 + number).start()
 
-    lax.fori_loop(10, 20, w_body, 0)
+    lax.fori_loop(12, 20, w_pass, 0)
 
     for unit in range(2):
         att_copy(x_down, unit, x_up, 0).wait_recv()
@@ -373,7 +416,7 @@
     att_copy(x_down, 0, x_up, 4).start()
     att_copy(x_up, 1, x_down, 5).start()
 
-    lax.fori_loop(20, 2 * CHIPS, w_body, 0)
+    lax.fori_loop(20, 30, w_pass, 0)
 
     x_far = ring(x, 2)
     load_w.wait()
@@ -399,6 +442,8 @@
         full = resid[rows].astype(jnp.float32)
         scale = lax.rsqrt(jnp.mean(full * full, axis=1, keepdims=True) + 1e-06)
         normed[rows] = (full * scale * mixer_gain[...]).astype(jnp.bfloat16)
+
+    lax.fori_loop(30, 2 * CHIPS, w_pass, 0)
 
     remote(weights.at[0], weights.at[0], pair_send.at[0], pair_recv.at[0], pair, x).wait_recv()
 
@@ -510,7 +555,10 @@
             pltpu.VMEM((64, HALF, 2 * DV), bf16),
             pltpu.VMEM((2, BLK, DV), bf16),
             pltpu.VMEM((2, 2, DV, BLK), bf16),
-            pltpu.VMEM((DV + SUMROWS, BLK), bf16),
+            pltpu.VMEM((2, DV + SUMROWS, BLK), bf16),
+            pltpu.VMEM((2, BLK, BLK), f32),
+            pltpu.VMEM((2, BLK, BLK), f32),
+            pltpu.VMEM((2, 2, 1, BLK), f32),
             pltpu.VMEM((2, 2, 1, BLK), f32),
             pltpu.VMEM((2, 2, DV + SUMROWS, BLK), f32),
             pltpu.VMEM((2, D, FFT), bf16),

time: 138 us -> 124 us (0.90)
  the two profiles are of different devices: /device:TPU:0 before, /device:TPU:9 now
where the time goes in v3:
time: 124 us
  Pallas kernels  122 us (98%)
  local copies, waits for them, and re-layouts  1.88 us (2%)
    pallas_call x1, Pallas kernels, per_device(): pl.pallas_call(layer_kernel, out_shape=jax.ShapeDtypeStruct(tokens.shape,...  122 us

profile of v3, /device:TPU:9, one launch (start us, length us, event | category | flops | bytes accessed | tf_op | source)
XLA Modules:
  0.0 123.7 jit_solution(13635530599559587731)
XLA Ops:
  0.0 121.9 %shard_map.100 = bf16[128,2048]{1,0:T(8,128)(2,1)} custom-call(bf16[128,2048]{1,0:T(8,128)(2,1)} %tokens.1, bf16[512,256]{1,0:T(8,128)(2,1)} %queries.1, bf16[512,256]{1,0:T(8,128)(2,1)} %keys.1, bf16[512,256]{1,0:T(8,128)(2,1)} %values.1, f32[2]{0:T(128)} %lambdas.1, f32[1,128]{1,0:T(1,128)} %bitcast.5, bf16[1024,2048]{1,0:T(8,128)(2,1)} %out_weight.1, ...), custom_call_target="tpu_custom_call" | custom-call | tf_op jit(solution)/shard_map/pallas_call | solution.py:549
  121.9 1.9 %copy.12 = bf16[128,2048]{1,0:T(8,128)(2,1)} copy(bf16[128,2048]{1,0:T(8,128)(2,1)} %shard_map.100) | data formatting | bytes 1048576

commit v4 on v3

--- a/solution.py
+++ b/solution.py
@@ -17,11 +17,17 @@
 FFT = 1024
 ROWS = 128
 SUMROWS = 16
-W_FROM = 26
+W_NEXT = 22
+W_A, W_B, W_C = 34 - W_NEXT, 16, 20
 
 HERE, LEFT, RIGHT, FAR = 0, 1, 2, 3
 FIRST = (HERE, LEFT, RIGHT, HERE, HERE, FAR, HERE, LEFT, LEFT, RIGHT, RIGHT, LEFT, RIGHT, FAR, FAR, FAR)
 SECOND = (HERE, HERE, HERE, LEFT, RIGHT, HERE, FAR, LEFT, RIGHT, LEFT, RIGHT, FAR, FAR, LEFT, RIGHT, FAR)
+
+OWN, SWAPPED = 0, 1
+KV_KIND = (OWN, SWAPPED, OWN, OWN, OWN, SWAPPED, SWAPPED, SWAPPED, OWN, OWN, SWAPPED, OWN, SWAPPED, SWAPPED, OWN, SWAPPED)
+KV_PLACE = (HERE, HERE, HERE, LEFT, RIGHT, HERE, LEFT, RIGHT, LEFT, RIGHT, FAR, FAR, LEFT, RIGHT, FAR, FAR)
+KV_MATE = (0, 0, 1, 0, 0, 1, 0, 0, 1, 1, 0, 0, 1, 1, 1, 1)
 
 
 def pick(index, table):
@@ -61,6 +67,8 @@
     result,
     kv,
     q_in,
+    q_given,
+    kv_given,
     q_t,
     v_t,
     scores_a,
@@ -83,6 +91,7 @@
     swap_sem,
     q_sem,
     kv_send,
+    kv_pair,
     kv_recv,
     w_send,
     w_recv,
@@ -90,8 +99,7 @@
     pair_recv,
     tok_send,
     tok_recv,
-    back_send,
-    back_recv,
+    back_sem,
     att_send,
     att_recv,
     sum_send,
@@ -103,8 +111,10 @@
     chip = sp // 2
     y = lax.rem(chip, RING)
     z = chip // RING
-    mirror = CHIPS - 1 - chip
+    mirror = 2 * CHIPS - 1 - sp
     pair = chip * 2 + (1 - core)
+    side = z // 2
+    mate_z = z + 1 - 2 * lax.rem(z, 2)
 
     def ring(place, step):
         return lax.rem(place + step, RING)
@@ -116,53 +126,52 @@
     z_up, z_down = at(y, ring(z, 1)), at(y, ring(z, 3))
     x_up, x_down = ring(x, 1), ring(x, 3)
 
+    mate, partner = at(y, mate_z), at(y, 3 - z)
+
     barrier = pltpu.get_barrier_semaphore()
-    greeted = [(s, x) for s in (y_up, y_down, z_up, z_down, pair, mirror * 2, mirror * 2 + 1)]
+    greeted = [(s, x) for s in (y_up, y_down, z_up, z_down, pair, mirror)]
     greeted += [(sp, x_up), (sp, x_down)]
     for device in greeted:
         pl.semaphore_signal(barrier, inc=1, device_id=device, device_id_type=MESH)
-    pl.semaphore_wait(barrier, len(greeted))
 
     def lanes(place):
         return pl.ds(pl.multiple_of(place * DV, DV), DV)
 
-    mine = lanes(core)
-    theirs = lanes(1 - core)
-    own_q = pltpu.make_async_copy(queries.at[:, pl.ds(0, DV)], q_in.at[0], own_sem.at[0])
-
-    def q_copy(head, slot, to):
-        return remote(
-            queries.at[:, pl.ds(head * DV, DV)], q_in.at[slot], q_sem.at[2 + head], q_sem.at[slot], to, x
-        )
-
-    @pl.when(core == 0)
-    def _():
-        q_copy(1, 0, pair).start()
-        own_q.start()
-
-    @pl.when(core == 1)
-    def _():
-        q_copy(0, 1, mirror * 2).start()
-        q_copy(1, 1, mirror * 2 + 1).start()
-
-    own_block = pl.ds((chip * 2 + core) * 2, 2)
-    pair_block = pl.ds((chip * 2 + 1 - core) * 2, 2)
+    kept, given = lanes(side), lanes(1 - side)
+    own_q = pltpu.make_async_copy(queries.at[:, kept], q_in.at[0], own_sem.at[0])
+    load_q = pltpu.make_async_copy(queries.at[:, given], q_given, own_sem.at[8])
+    swap_q = remote(q_given, q_in.at[1], q_sem.at[0], q_sem.at[1], mirror, x)
     swaps = []
     owns = []
+    loads = [load_q]
     for number, (array, half) in enumerate(((keys, pl.ds(0, DV)), (values, pl.ds(DV, DV)))):
         for unit in range(2):
             rows = pl.ds(unit * HALF, HALF)
-            place = kv.at[(chip * 2 + core) * 2 + unit, :, half]
+            place = kv.at[sp * 2 + unit, :, half]
             index = number * 2 + unit
+            held = kv_given.at[unit, :, half]
+            loads.append(pltpu.make_async_copy(array.at[rows, given], held, own_sem.at[9 + index]))
             swaps.append(
-                remote(array.at[rows, theirs], place, swap_sem.at[4 + index], swap_sem.at[index], pair, x)
+                remote(held, place, swap_sem.at[4 + index], swap_sem.at[index], partner, x)
             )
-            owns.append(pltpu.make_async_copy(array.at[rows, mine], place, own_sem.at[1 + index]))
-    for copy in swaps + owns:
+            owns.append(pltpu.make_async_copy(array.at[rows, kept], place, own_sem.at[1 + index]))
+    own_tok = pltpu.make_async_copy(tokens, tok.at[x], own_sem.at[5])
+    for copy in loads + owns + [own_q, own_tok]:
         copy.start()
 
-    own_tok = pltpu.make_async_copy(tokens, tok.at[x], own_sem.at[5])
-    own_tok.start()
+    run_max[...] = jnp.full(run_max.shape, -1e30, jnp.float32)
+    acc[...] = jnp.zeros(acc.shape, jnp.float32)
+    v_t[...] = jnp.ones(v_t.shape, jnp.bfloat16)
+    scores_b[...] = jnp.full(scores_b.shape, -1e30, jnp.float32)
+    top[...] = jnp.full(top.shape, -1e30, jnp.float32)
+
+    pl.semaphore_wait(barrier, len(greeted))
+
+    for copy in loads:
+        copy.wait()
+    for copy in swaps:
+        copy.start()
+    swap_q.start()
 
     def tok_copy(source, unit, to, fwd):
         rows = pl.ds(unit * (ROWS // 2), ROWS // 2)
@@ -182,21 +191,8 @@
     load_w = pltpu.make_async_copy(out_weight, out_w, load_sem.at[0])
     load_w.start()
 
-    run_max[...] = jnp.full(run_max.shape, -1e30, jnp.float32)
-    acc[...] = jnp.zeros(acc.shape, jnp.float32)
-    v_t[...] = jnp.ones(v_t.shape, jnp.bfloat16)
-    scores_b[...] = jnp.full(scores_b.shape, -1e30, jnp.float32)
-    top[...] = jnp.full(top.shape, -1e30, jnp.float32)
-
-    own_tok.wait()
-    for unit in range(2):
-        for number, to in enumerate((x_up, x_down)):
-            tok_copy(x, unit, to, unit * 2 + number).start()
-
     for copy in owns:
         copy.wait()
-    for copy in swaps:
-        copy.wait_recv()
 
     def item_of(number):
         odd = lax.rem(number, 2)
@@ -245,28 +241,95 @@
             def _(unit=unit, to=to):
                 copy(unit, to).start()
 
-    def kv_ref(odd, source, unit):
-        first = (source * 2 + odd) * 2
-        return kv.at[pl.ds(first, 2)] if unit is None else kv.at[first + unit]
-
-    def kv_sem(odd, source, unit):
-        return kv_recv.at[(source * 2 + odd) * 2 + unit]
+    def kv_item(number):
+        kind = pick(number, KV_KIND)
+        by_mate = pick(number, KV_MATE)
+        place = pick(number, KV_PLACE)
+        through = jnp.where(by_mate == 1, mate_z, z)
+        source_z = jnp.where(kind == OWN, through, 3 - through)
+        return kind, place, by_mate, source_z * RING + ring(y, shift(place))
 
     def kv_pass(number, carry):
-        pass_on(number, kv_ref, kv_send.at[0], kv_sem)
+        kind, place, by_mate, source = kv_item(number)
+        block = source * 2 + core
+
+        def copy(unit, to, send_sem=kv_send.at[0]):
+            ref = kv.at[pl.ds(block * 2, 2)] if unit is None else kv.at[block * 2 + unit]
+            recv_sem = kv_recv.at[block * 2 + (0 if unit is None else unit)]
+            return remote(ref, ref, send_sem, recv_sem, to, x)
+
+        direct = (kind == OWN) | (by_mate == 0)
+        swapped_in = (kind == SWAPPED) & (place == HERE) & (by_mate == 0)
+        halves = direct & (place == FAR)
+
+        @pl.when(swapped_in)
+        def _():
+            for copied in swaps:
+                copied.wait_recv()
+
+        @pl.when(halves)
+        def _():
+            copy(0, sp).wait_recv()
+            copy(1, sp).wait_recv()
+
+        @pl.when(jnp.logical_not(swapped_in | halves | (number == 0)))
+        def _():
+            copy(None, sp).wait_recv()
+
+        to_mate = (by_mate == 0) & ((kind == SWAPPED) | (place == HERE))
+        for unit, to, sends in (
+            (None, y_up, direct & (place == HERE)),
+            (None, y_down, direct & (place == HERE)),
+            (0, y_up, direct & (place == LEFT)),
+            (1, y_down, direct & (place == RIGHT)),
+            (None, mate, to_mate),
+        ):
+
+            @pl.when(sends)
+            def _(unit=unit, to=to):
+                copy(unit, to).start()
+
+        copy(None, pair, kv_pair.at[0]).start()
         return carry
 
-    lax.fori_loop(0, 2, kv_pass, 0)
-
-    @pl.when(core == 0)
-    def _():
-        own_q.wait()
-
-    @pl.when(core == 1)
-    def _():
-        q_copy(0, 0, pair).wait_recv()
-
-    q_copy(0, 1, mirror * 2).wait_recv()
+    def w_ref(odd, source, unit):
+        row = source * 128 + core * 64
+        if unit is None:
+            return weights.at[odd, pl.ds(pl.multiple_of(row, 64), 64)]
+        return weights.at[odd, pl.ds(pl.multiple_of(row + unit * 32, 32), 32)]
+
+    def w_sem(odd, source, unit):
+        return w_recv.at[odd, source * 2 + unit]
+
+    def w_own(odd, to):
+        item = w_ref(odd, chip, None)
+        remote(item, item, w_send.at[0], w_sem(odd, chip, 0), to, x).start()
+
+    def w_pass(number, carry):
+        pass_on(number, w_ref, w_send.at[0], w_sem)
+        odd, _, _, source = item_of(number)
+        item = w_ref(odd, source, None)
+        remote(item, item, pair_send.at[0], pair_recv.at[0], pair, x).start()
+        return carry
+
+    kv_pass(jnp.int32(0), 0)
+    for copy in own_w:
+        copy.wait()
+    for odd in range(2):
+        for to in (y_up, y_down, mate):
+            w_own(odd, to)
+        item = w_ref(odd, chip, None)
+        remote(item, item, pair_send.at[0], pair_recv.at[0], pair, x).start()
+    own_tok.wait()
+    for unit in range(2):
+        for number, to in enumerate((x_up, x_down)):
+            tok_copy(x, unit, to, unit * 2 + number).start()
+    kv_pass(jnp.int32(1), 0)
+    for odd in range(2):
+        w_own(odd, partner)
+    kv_pass(jnp.int32(2), 0)
+    own_q.wait()
+    swap_q.wait_recv()
 
     for slot in range(2):
         q_slot = (q_in[slot].astype(jnp.float32) * DQK ** -0.5).T.astype(jnp.bfloat16)
@@ -275,22 +338,6 @@
         q_t[slot, 0, DQK:] = zero
         q_t[slot, 1, :DQK] = zero
         q_t[slot, 1, DQK:] = q_slot[DQK:]
-
-    def w_ref(odd, source, unit):
-        row = source * 128 + core * 64
-        if unit is None:
-            return weights.at[odd, pl.ds(pl.multiple_of(row, 64), 64)]
-        return weights.at[odd, pl.ds(pl.multiple_of(row + unit * 32, 32), 32)]
-
-    def w_sem(odd, source, unit):
-        return w_recv.at[odd, source * 2 + unit]
-
-    def w_pass(number, carry):
-        pass_on(number, w_ref, w_send.at[0], w_sem)
-        odd, _, _, source = item_of(number)
-        item = w_ref(odd, source, None)
-        remote(item, item, pair_send.at[0], pair_recv.at[0], pair, x).start()
-        return carry
 
     scores_of = (scores_a, scores_b)
 
@@ -322,13 +369,23 @@
             absorb(before, j, weight, new_max, last_slot)
 
     def kv_body(number, carry):
-        @pl.when(number >= 2)
-        def _():
-            kv_pass(number, 0)
-
-        @pl.when(number >= W_FROM)
-        def _():
-            w_pass(number - W_FROM, 0)
+        item = number // 2
+        passed = lax.rem(number, 2)
+        _, _, _, source = kv_item(item)
+        block = source * 2 + jnp.where(passed == 1, 1 - core, core)
+
+        @pl.when((passed == 0) & (item >= 3))
+        def _():
+            kv_pass(item, 0)
+
+        @pl.when(passed == 1)
+        def _():
+            ref = kv.at[pl.ds(block * 2, 2)]
+            remote(ref, ref, kv_send.at[0], kv_recv.at[block * 2], pair, x).wait_recv()
+
+        @pl.when(number >= W_NEXT)
+        def _():
+            w_pass(number - W_NEXT + 2, 0)
 
         @pl.when(number == 10)
         def _():
@@ -338,12 +395,9 @@
             tok_copy(x_down, 0, x_up, 4).start()
             tok_copy(x_up, 1, x_down, 5).start()
 
-        odd, _, _, source = item_of(number)
-        block = source * 2 + odd
-
         def slot_body(slot, inner):
             now, last_slot = inner
-            q_block = jnp.where(slot == 0, chip * 2, 31 - chip * 2)
+            q_block = jnp.where(slot == 0, sp, mirror)
             for parity in range(2):
                 for masked in (False, True):
                     wanted = (block == q_block) if masked else (block < q_block)
@@ -357,73 +411,71 @@
 
         return lax.fori_loop(0, 2, slot_body, carry)
 
-    for copy in own_w:
-        copy.wait()
     _, last_slot = lax.fori_loop(0, 2 * CHIPS, kv_body, (jnp.int32(0), jnp.int32(0)))
     for j in range(2):
         weight, new_max = softmax(0, j, last_slot)
         absorb(0, j, weight, new_max, last_slot)
 
-    for slot in range(2):
+    def att_lanes(source, part):
+        head = side if part == 0 else 1 - side
+        return pl.ds(pl.multiple_of((source * 2 + head) * DV, DV), DV)
+
+    back = remote(
+        stage, att.at[:, att_lanes(x, 0)], back_sem.at[0], back_sem.at[1], mirror, x
+    )
+
+    for slot in (1, 0):
         map_1 = acc[slot, 0, :DV] / acc[slot, 0, DV : DV + 1]
         map_2 = acc[slot, 1, :DV] / acc[slot, 1, DV : DV + 1]
-        lam = jnp.where(core == 0, lambdas[0], lambdas[1])
+        lam = jnp.where(side == 0, lambdas[0], lambdas[1])
         differ = map_1 - lam * map_2
         spread = lax.rsqrt(jnp.mean(differ * differ, axis=0, keepdims=True) + 1e-06)
-        stage[slot] = ((differ * spread).T * head_gain[...]).astype(jnp.bfloat16)
-
-    def att_lanes(head):
-        return pl.ds(pl.multiple_of((x * 2 + head) * DV, DV), DV)
-
-    def back_copy(slot, head, to):
+        attended = ((differ * spread).T * head_gain[...]).astype(jnp.bfloat16)
+        if slot == 1:
+            stage[...] = attended
+            back.start()
+        else:
+            att[:, att_lanes(x, 0)] = attended
+
+    def att_copy(source, part, unit, to, sem):
+        place = att.at[pl.ds(unit * HALF, HALF), att_lanes(source, part)]
         return remote(
-            stage.at[slot], att.at[:, att_lanes(head)], back_send.at[slot], back_recv.at[head], to, x
-        )
-
-    @pl.when(core == 0)
-    def _():
-        att[:, att_lanes(0)] = stage[0]
-
-    @pl.when(core == 1)
-    def _():
-        back_copy(0, 1, pair).start()
-
-    back_copy(1, core, mirror * 2 + 1).start()
-
-    lax.fori_loop(2 * CHIPS - W_FROM, 12, w_pass, 0)
-
-    @pl.when(core == 1)
-    def _():
-        back_copy(0, 0, pair).wait_recv()
-
-    back_copy(0, 1, pair).wait_recv()
-
-    def att_copy(source, unit, to, sem):
-        place = att.at[
-            pl.ds(unit * HALF, HALF), pl.ds(pl.multiple_of(source * 2 * DV, 2 * DV), 2 * DV)
-        ]
-        return remote(place, place, att_send.at[sem], att_recv.at[source, unit], sp, to)
-
-    for unit in range(2):
-        for number, to in enumerate((x_up, x_down)):
-            att_copy(x, unit, to, unit * 2 + number).start()
-
-    lax.fori_loop(12, 20, w_pass, 0)
-
-    for unit in range(2):
-        att_copy(x_down, unit, x_up, 0).wait_recv()
-        att_copy(x_up, unit, x_down, 0).wait_recv()
-    att_copy(x_down, 0, x_up, 4).start()
-    att_copy(x_up, 1, x_down, 5).start()
-
-    lax.fori_loop(20, 30, w_pass, 0)
+            place, place, att_send.at[part * 6 + sem], att_recv.at[source, part * 2 + unit], sp, to
+        )
+
+    def att_begin(part):
+        for unit in range(2):
+            for number, to in enumerate((x_up, x_down)):
+                att_copy(x, part, unit, to, unit * 2 + number).start()
+
+    def att_forward(part):
+        for unit in range(2):
+            att_copy(x_down, part, unit, x_up, 0).wait_recv()
+            att_copy(x_up, part, unit, x_down, 0).wait_recv()
+        att_copy(x_down, part, 0, x_up, 4).start()
+        att_copy(x_up, part, 1, x_down, 5).start()
+
+    att_begin(0)
+
+    lax.fori_loop(W_A, W_B, w_pass, 0)
+
+    back.wait_recv()
+    att_begin(1)
+    att_forward(0)
+
+    lax.fori_loop(W_B, W_C, w_pass, 0)
+
+    att_forward(1)
+
+    lax.fori_loop(W_C, 22, w_pass, 0)
 
     x_far = ring(x, 2)
     load_w.wait()
     for unit in range(2):
         tok_copy(x_far, unit, x_up, 0).wait_recv()
     for unit in range(2):
-        att_copy(x_far, unit, x_up, 0).wait_recv()
+        for piece in range(2):
+            att_copy(x_far, piece, unit, x_up, 0).wait_recv()
 
     @pl.loop(0, 4)
     def _(column):
@@ -435,6 +487,8 @@
         resid[:, cols] = (tok_cols.astype(jnp.float32) + projected.astype(jnp.float32)).astype(
             jnp.bfloat16
         )
+        w_pass(22 + 2 * column, 0)
+        w_pass(23 + 2 * column, 0)
 
     @pl.loop(0, 8)
     def _(tile):
@@ -482,12 +536,14 @@
         part[0, half] = down(hidden, half * wide, wide).astype(jnp.bfloat16)
         relay_copy(half, to).start()
 
+    near = []
     for number, to in ((0, x_up), (1, x_down)):
-        hidden = hidden_of(to)
         plain = 1 - number
-        part[1 + number, plain] = down(hidden, plain * wide, wide).astype(jnp.bfloat16)
+        near.append(hidden_of(to))
+        part[1 + number, plain] = down(near[number], plain * wide, wide).astype(jnp.bfloat16)
         final_copy(number, plain, to).start()
-        added = down(hidden, number * wide, wide)
+    for number, to in ((0, x_up), (1, x_down)):
+        added = down(near[number], number * wide, wide)
         relay_copy(number, to).wait_recv()
         part[1 + number, number] = (added + relay[number].astype(jnp.float32)).astype(jnp.bfloat16)
         final_copy(number, number, to).start()
@@ -502,27 +558,21 @@
             total = total + arrived[number, half].astype(jnp.float32)
         result[:, cols] = total.astype(jnp.bfloat16)
 
-    @pl.when(core == 0)
-    def _():
-        q_copy(1, 0, pair).wait_send()
-
-    @pl.when(core == 1)
-    def _():
-        q_copy(0, 1, mirror * 2).wait_send()
-        q_copy(1, 1, mirror * 2 + 1).wait_send()
-        back_copy(0, 1, pair).wait_send()
-
+    swap_q.wait_send()
+    back.wait_send()
     for copy in swaps:
         copy.wait_send()
     for sem in range(6):
         tok_copy(x, 0, x_up, sem).wait_send()
-        att_copy(x, 0, x_up, sem).wait_send()
-    sent_kv = kv.at[pl.ds(0, 60)]
+        for piece in range(2):
+            att_copy(x, piece, 0, x_up, sem).wait_send()
+    sent_kv = kv.at[pl.ds(0, 28)]
     remote(sent_kv, sent_kv, kv_send.at[0], kv_recv.at[0], y_up, x).wait_send()
+    sent_kv = kv.at[pl.ds(0, 32)]
+    remote(sent_kv, sent_kv, kv_pair.at[0], kv_recv.at[0], pair, x).wait_send()
     sent_w = weights.at[0, pl.ds(0, 60 * 32)]
     remote(sent_w, sent_w, w_send.at[0], w_recv.at[0, 0], y_up, x).wait_send()
     remote(weights.at[0], weights.at[0], pair_send.at[0], pair_recv.at[0], pair, x).wait_send()
-    back_copy(1, core, mirror * 2 + 1).wait_send()
     for number in range(2):
         relay_copy(number, x_up).wait_send()
         for half in range(2):
@@ -554,6 +604,8 @@
         scratch_shapes=[
             pltpu.VMEM((64, HALF, 2 * DV), bf16),
             pltpu.VMEM((2, BLK, DV), bf16),
+            pltpu.VMEM((BLK, DV), bf16),
+            pltpu.VMEM((2, HALF, 2 * DV), bf16),
             pltpu.VMEM((2, 2, DV, BLK), bf16),
             pltpu.VMEM((2, DV + SUMROWS, BLK), bf16),
             pltpu.VMEM((2, BLK, BLK), f32),
@@ -564,17 +616,18 @@
             pltpu.VMEM((2, D, FFT), bf16),
             pltpu.VMEM((1024, D), bf16),
             pltpu.VMEM((TP, ROWS, D), bf16),
-            pltpu.VMEM((2, BLK, DV), bf16),
+            pltpu.VMEM((BLK, DV), bf16),
             pltpu.VMEM((BLK, 1024), bf16),
             pltpu.VMEM((BLK, D), bf16),
             pltpu.VMEM((BLK, D), bf16),
             pltpu.VMEM((3, 2, ROWS, D // 2), bf16),
             pltpu.VMEM((2, ROWS, D // 2), bf16),
             pltpu.VMEM((2, 2, ROWS, D // 2), bf16),
-            dma((8,)),
+            dma((13,)),
             dma((1,)),
             dma((8,)),
-            dma((4,)),
+            dma((2,)),
+            dma((1,)),
             dma((1,)),
             dma((64,)),
             dma((1,)),
@@ -584,9 +637,8 @@
             dma((6,)),
             dma((TP, 2)),
             dma((2,)),
-            dma((2,)),
-            dma((6,)),
-            dma((TP, 2)),
+            dma((12,)),
+            dma((TP, 4)),
             dma((6,)),
             dma((6,)),
         ],

time: 124 us -> 107 us (0.86)
  the two profiles are of different devices: /device:TPU:9 before, /device:TPU:0 now
where the time goes in v4:
time: 107 us; the launch traced here: 105 us
  Pallas kernels  103 us (96%)
  local copies, waits for them, and re-layouts  1.88 us (2%)
    pallas_call x1, Pallas kernels, per_device(): pl.pallas_call(layer_kernel, out_shape=jax.ShapeDtypeStruct(tokens.shape,...  103 us

profile of v4, /device:TPU:0, one launch (start us, length us, event | category | flops | bytes accessed | tf_op | source)
XLA Modules:
  0.0 105.3 jit_solution(13077210528175635323)
XLA Ops:
  0.0 103.4 %shard_map.100 = bf16[128,2048]{1,0:T(8,128)(2,1)} custom-call(bf16[128,2048]{1,0:T(8,128)(2,1)} %tokens.1, bf16[512,256]{1,0:T(8,128)(2,1)} %queries.1, bf16[512,256]{1,0:T(8,128)(2,1)} %keys.1, bf16[512,256]{1,0:T(8,128)(2,1)} %values.1, f32[2]{0:T(128)} %lambdas.1, f32[1,128]{1,0:T(1,128)} %bitcast.5, bf16[1024,2048]{1,0:T(8,128)(2,1)} %out_weight.1, ...), custom_call_target="tpu_custom_call" | custom-call | tf_op jit(solution)/shard_map/pallas_call | solution.py:599
  103.4 1.9 %copy.12 = bf16[128,2048]{1,0:T(8,128)(2,1)} copy(bf16[128,2048]{1,0:T(8,128)(2,1)} %shard_map.100) | data formatting | bytes 1048576

commit v5 on v4

--- a/solution.py
+++ b/solution.py
@@ -18,7 +18,7 @@
 ROWS = 128
 SUMROWS = 16
 W_NEXT = 22
-W_A, W_B, W_C = 34 - W_NEXT, 16, 20
+W_A, W_B, W_C, W_P = 34 - W_NEXT, 22, 24, 24
 
 HERE, LEFT, RIGHT, FAR = 0, 1, 2, 3
 FIRST = (HERE, LEFT, RIGHT, HERE, HERE, FAR, HERE, LEFT, LEFT, RIGHT, RIGHT, LEFT, RIGHT, FAR, FAR, FAR)
@@ -28,6 +28,9 @@
 KV_KIND = (OWN, SWAPPED, OWN, OWN, OWN, SWAPPED, SWAPPED, SWAPPED, OWN, OWN, SWAPPED, OWN, SWAPPED, SWAPPED, OWN, SWAPPED)
 KV_PLACE = (HERE, HERE, HERE, LEFT, RIGHT, HERE, LEFT, RIGHT, LEFT, RIGHT, FAR, FAR, LEFT, RIGHT, FAR, FAR)
 KV_MATE = (0, 0, 1, 0, 0, 1, 0, 0, 1, 1, 0, 0, 1, 1, 1, 1)
+
+KV_CODE = tuple(k + 2 * m + 4 * p for k, m, p in zip(KV_KIND, KV_MATE, KV_PLACE))
+W_CODE = tuple(f + 4 * s for f, s in zip(FIRST, SECOND))
 
 
 def pick(index, table):
@@ -196,15 +199,15 @@
 
     def item_of(number):
         odd = lax.rem(number, 2)
-        first = pick(number // 2, FIRST)
-        second = pick(number // 2, SECOND)
+        code = pick(number // 2, W_CODE)
+        first, second = lax.rem(code, 4), code // 4
         y_step = jnp.where(odd == 0, shift(first), shift(second))
         z_step = jnp.where(odd == 0, shift(second), shift(first))
         source = ring(z, z_step) * RING + ring(y, y_step)
         return odd, first, second, source
 
     def pass_on(number, ref_of, send_sem, recv_of):
-        odd, first, second, source = item_of(number)
+        odd, first, second, source = decoded = item_of(number)
         first_up = jnp.where(odd == 0, y_up, z_up)
         first_down = jnp.where(odd == 0, y_down, z_down)
         second_up = jnp.where(odd == 0, z_up, y_up)
@@ -241,16 +244,19 @@
             def _(unit=unit, to=to):
                 copy(unit, to).start()
 
+        return decoded
+
     def kv_item(number):
-        kind = pick(number, KV_KIND)
-        by_mate = pick(number, KV_MATE)
-        place = pick(number, KV_PLACE)
+        code = pick(number, KV_CODE)
+        kind = lax.rem(code, 2)
+        by_mate = lax.rem(code // 2, 2)
+        place = code // 4
         through = jnp.where(by_mate == 1, mate_z, z)
         source_z = jnp.where(kind == OWN, through, 3 - through)
         return kind, place, by_mate, source_z * RING + ring(y, shift(place))
 
-    def kv_pass(number, carry):
-        kind, place, by_mate, source = kv_item(number)
+    def kv_pass(number, item):
+        kind, place, by_mate, source = item
         block = source * 2 + core
 
         def copy(unit, to, send_sem=kv_send.at[0]):
@@ -290,7 +296,6 @@
                 copy(unit, to).start()
 
         copy(None, pair, kv_pair.at[0]).start()
-        return carry
 
     def w_ref(odd, source, unit):
         row = source * 128 + core * 64
@@ -306,13 +311,12 @@
         remote(item, item, w_send.at[0], w_sem(odd, chip, 0), to, x).start()
 
     def w_pass(number, carry):
-        pass_on(number, w_ref, w_send.at[0], w_sem)
-        odd, _, _, source = item_of(number)
+        odd, _, _, source = pass_on(number, w_ref, w_send.at[0], w_sem)
         item = w_ref(odd, source, None)
         remote(item, item, pair_send.at[0], pair_recv.at[0], pair, x).start()
         return carry
 
-    kv_pass(jnp.int32(0), 0)
+    kv_pass(jnp.int32(0), kv_item(jnp.int32(0)))
     for copy in own_w:
         copy.wait()
     for odd in range(2):
@@ -324,10 +328,10 @@
     for unit in range(2):
         for number, to in enumerate((x_up, x_down)):
             tok_copy(x, unit, to, unit * 2 + number).start()
-    kv_pass(jnp.int32(1), 0)
+    kv_pass(jnp.int32(1), kv_item(jnp.int32(1)))
     for odd in range(2):
         w_own(odd, partner)
-    kv_pass(jnp.int32(2), 0)
+    kv_pass(jnp.int32(2), kv_item(jnp.int32(2)))
     own_q.wait()
     swap_q.wait_recv()
 
@@ -371,12 +375,12 @@
     def kv_body(number, carry):
         item = number // 2
         passed = lax.rem(number, 2)
-        _, _, _, source = kv_item(item)
-        block = source * 2 + jnp.where(passed == 1, 1 - core, core)
+        decoded = kv_item(item)
+        block = decoded[3] * 2 + jnp.where(passed == 1, 1 - core, core)
 
         @pl.when((passed == 0) & (item >= 3))
         def _():
-            kv_pass(item, 0)
+            kv_pass(item, decoded)
 
         @pl.when(passed == 1)
         def _():
@@ -467,7 +471,7 @@
 
     att_forward(1)
 
-    lax.fori_loop(W_C, 22, w_pass, 0)
+    lax.fori_loop(W_C, W_P, w_pass, 0)
 
     x_far = ring(x, 2)
     load_w.wait()
@@ -487,8 +491,8 @@
         resid[:, cols] = (tok_cols.astype(jnp.float32) + projected.astype(jnp.float32)).astype(
             jnp.bfloat16
         )
-        w_pass(22 + 2 * column, 0)
-        w_pass(23 + 2 * column, 0)
+        w_pass(W_P + 2 * column, 0)
+        w_pass(W_P + 1 + 2 * column, 0)
 
     @pl.loop(0, 8)
     def _(tile):
@@ -497,7 +501,7 @@
         scale = lax.rsqrt(jnp.mean(full * full, axis=1, keepdims=True) + 1e-06)
         normed[rows] = (full * scale * mixer_gain[...]).astype(jnp.bfloat16)
 
-    lax.fori_loop(30, 2 * CHIPS, w_pass, 0)
+    lax.fori_loop(W_P + 8, 2 * CHIPS, w_pass, 0)
 
     remote(weights.at[0], weights.at[0], pair_send.at[0], pair_recv.at[0], pair, x).wait_recv()
 

time: 107 us -> 106 us (level); the launches traced: 105 us -> 106 us
  no operation moved by 1% of the time
where the time goes in v5:
time: 106 us
  Pallas kernels  104 us (98%)
  local copies, waits for them, and re-layouts  1.88 us (2%)
    pallas_call x1, Pallas kernels, per_device(): pl.pallas_call(layer_kernel, out_shape=jax.ShapeDtypeStruct(tokens.shape,...  104 us

profile of v5, /device:TPU:0, one launch (start us, length us, event | category | flops | bytes accessed | tf_op | source)
XLA Modules:
  0.0 105.7 jit_solution(14854806953146556894)
XLA Ops:
  0.0 103.8 %shard_map.100 = bf16[128,2048]{1,0:T(8,128)(2,1)} custom-call(bf16[128,2048]{1,0:T(8,128)(2,1)} %tokens.1, bf16[512,256]{1,0:T(8,128)(2,1)} %queries.1, bf16[512,256]{1,0:T(8,128)(2,1)} %keys.1, bf16[512,256]{1,0:T(8,128)(2,1)} %values.1, f32[2]{0:T(128)} %lambdas.1, f32[1,128]{1,0:T(1,128)} %bitcast.5, bf16[1024,2048]{1,0:T(8,128)(2,1)} %out_weight.1, ...), custom_call_target="tpu_custom_call" | custom-call | tf_op jit(solution)/shard_map/pallas_call | solution.py:603
  103.8 1.9 %copy.12 = bf16[128,2048]{1,0:T(8,128)(2,1)} copy(bf16[128,2048]{1,0:T(8,128)(2,1)} %shard_map.100) | data formatting | bytes 1048576
